TPU v7x, 256 devices: a whole 4x4x8 slice. The times are simulated.
256 devices in a mesh: sp: 32 (over z, x), tp: 8 (over y, core).
Axes of the slice: x: 4, y: 4, z: 8, core: 2. Of those that a mesh axis runs over, the one named last changes fastest.
Arguments:
- inputs: bfloat16 [12288, 2048], P('sp', 'tp'), may hold values from -6 to 6
- norm_gain: float32 [2048], replicated, may hold values from 0.1 to 1.9
- query_weight: bfloat16 [2048, 1024], P(None, 'tp')
- key_weight: bfloat16 [2048, 1024], P(None, 'tp'), may hold values from -0.15625 to 0.15625
- value_weight: bfloat16 [2048, 1024], P(None, 'tp'), may hold values from -0.125 to 0.125
- memory_query_weight: bfloat16 [2048, 1024], P(None, 'tp'), may hold values from -0.125 to 0.125
- memory_key_weight: bfloat16 [2048, 1024], P(None, 'tp'), may hold values from -0.125 to 0.125
- memory_value_weight: bfloat16 [2048, 1024], P(None, 'tp'), may hold values from -0.125 to 0.125
- input_gate_weight: bfloat16 [2048, 16], P(None, 'tp')
- forget_gate_weight: bfloat16 [2048, 16], P(None, 'tp'), may hold values from -0.3125 to 0.3125
- forget_bias: float32 [16], P('tp'), may hold values from 3 to 13
- decay_shift: float32 [12288, 16], P('sp', 'tp'), may hold values from -2 to 0, as said below
- lambdas: float32 [16], P('tp'), may hold values from 0.3 to 0.8
- head_gain: float32 [64], replicated, may hold values from 0.1 to 1.9
- out_weight_attention: bfloat16 [1024, 2048], P('tp'), may hold values from -0.125 to 0.125
- out_weight_memory: bfloat16 [1024, 2048], P('tp'), may hold values from -0.125 to 0.125
Outputs:
- combined: bfloat16 [12288, 2048], P('sp', 'tp')
Inputs may be any that keep to these rules, and one draw needn't show every extreme that they name: `decay_shift`: never positive.
All inputs are finite; a program needn't handle non-finite values.
Results may differ from a plain program's by a relative error of at most 0.018.
The roundings to bfloat16 on the way count: a program that leaves them out, or rounds other values in their place, can miss the bound.
Values may be sent and summed in bfloat16 or wider, within the bound.
A program may use at most 192 MiB of HBM per device.

v0:
```python
import jax
import jax.numpy as jnp
from jax import lax
from jax.sharding import Mesh
from jax.sharding import PartitionSpec as P

HEAD = 64
DD = 32
BLOCK = 64
SP = ("sp_0", "sp_1")


EPSILON = 1e-06
ROTARY_BASE = 10000.0
NEGATIVE = -1e30


def joined_along(pieces, dim):
    lengths = list(pieces.shape[1:])
    lengths[dim] *= pieces.shape[0]
    return jnp.moveaxis(pieces, 0, dim).reshape(lengths)


def from_everyone(array, axis):
    devices = lax.axis_size(axis)
    return lax.all_to_all(
        jnp.broadcast_to(array[None], (devices, *array.shape)), axis, 0, 0, tiled=True
    )


def gather_directly(array, axis, dim):
    return joined_along(from_everyone(array, axis), dim)


def gather_axes(array, axes, dim):
    filled = array
    for number in range(len(axes) - 1, -1, -1):
        filled = lax.all_gather(filled, axes[number], axis=dim, tiled=True)
    return filled


def all_in_one(array, axis):
    leaves = jax.tree.leaves(array)
    sequence = sorted(range(len(leaves)), key=lambda k: -leaves[k].size)
    width = (1, *leaves[sequence[0]].shape)[-1]
    lines = [
        jnp.pad(leaves[k].reshape(-1), (0, -leaves[k].size % width)).reshape(-1, width)
        for k in sequence
    ]
    both, at, found = (from_everyone(jnp.concatenate(lines), axis), 0, {})
    for k, line in zip(sequence, lines):
        piece = both[:, at : at + len(line)].reshape(len(both), -1)
        found[k] = piece[:, : leaves[k].size].reshape(-1, *leaves[k].shape)
        at += len(line)
    numbers = iter(range(len(leaves)))
    return jax.tree.map(lambda _: found[next(numbers)], array)


def combined_pairwise(pieces, combine):
    while len(jax.tree.leaves(pieces)[0]) > 1:
        pieces = jax.vmap(combine)(
            *(jax.tree.map(lambda part: part[side::2], pieces) for side in (0, 1))
        )
    return jax.tree.map(lambda part: part[0], pieces)


def carried_in(array, axis, combine, identity):
    devices, mine = (lax.axis_size(axis), lax.axis_index(axis))
    passed = jnp.arange(devices) < mine

    def kept(part, zero, own):
        part = jnp.where(
            passed.reshape(-1, *(1 for _ in own.shape)), part, jnp.asarray(zero, own.dtype)
        )
        return part

    pieces = all_in_one(array, axis)
    return combined_pairwise(jax.tree.map(kept, pieces, identity, array), combine)


def split_up(array, dim, devices):
    before, after = (array.shape[:dim], array.shape[dim + 1 :])
    return jnp.moveaxis(array.reshape(*before, devices, -1, *after), dim, 0)


def sum_at_owner(array, axis, dim):
    pieces = split_up(array, dim, lax.axis_size(axis))
    arrived = lax.all_to_all(pieces, axis, split_axis=0, concat_axis=0, tiled=True)
    return arrived.astype(jnp.float32).sum(axis=0)


def rotate(halves, positions):
    middle = halves.shape[-1] // 2
    inverse = 1.0 / ROTARY_BASE ** (jnp.arange(middle, dtype=jnp.float32) / middle)
    angles = positions.astype(jnp.float32)[:, None] * inverse[None, :]
    cosine = jnp.cos(angles)[:, None, :]
    sine_part = jnp.sin(angles)[:, None, :]
    floats = halves.astype(jnp.float32)
    former = floats[..., :middle]
    latter = floats[..., middle:]
    turned = jnp.concatenate(
        [former * cosine - latter * sine_part, latter * cosine + former * sine_part], axis=-1
    )
    return turned.astype(jnp.bfloat16)


def advance_state(carried, block_entry):
    memory, normal, stable = carried
    block_memory, block_normal, block_max, block_decay = block_entry
    new_stable = jnp.maximum(block_decay + stable, block_max)
    former = jnp.exp(block_decay + stable - new_stable)
    latter = jnp.exp(block_max - new_stable)
    return (
        former[:, None, None] * memory + latter[:, None, None] * block_memory,
        former[:, None] * normal + latter[:, None] * block_normal,
        new_stable,
    )


def memory_blocks(queries, key_heads, values, gate_in, log_forget, entering):
    token_count, head_count, head_width = queries.shape
    block_count = token_count // BLOCK
    highest = lax.Precision.HIGHEST

    def blocked(flat_array):
        return (
            flat_array.astype(jnp.float32)
            .reshape(block_count, BLOCK, head_count, head_width)
            .transpose(2, 0, 1, 3)
        )

    query_blocks = blocked(queries)
    key_blocks = blocked(key_heads) * head_width ** (-0.5)
    value_blocks = blocked(values)
    gate_blocks = gate_in.reshape(block_count, BLOCK, head_count).transpose(2, 0, 1)
    cumulative = jnp.cumsum(
        log_forget.reshape(block_count, BLOCK, head_count).transpose(2, 0, 1), axis=-1
    )
    block_ends = cumulative[..., -1]
    toward_end = block_ends[..., None] - cumulative + gate_blocks
    local_max = jnp.max(toward_end, axis=-1)
    end_weights = jnp.exp(toward_end - local_max[..., None])
    local_memory = jnp.einsum(
        "hcl,hclv,hclk->chvk", end_weights, value_blocks, key_blocks, precision=highest
    )
    local_normal = jnp.einsum("hcl,hclk->chk", end_weights, key_blocks, precision=highest)

    def scan_step(carried, block_entry):
        return (advance_state(carried, block_entry), carried)

    entries = (local_memory, local_normal, local_max.T, block_ends.T)
    unused, (memory_in, normal_in, stable_in) = lax.scan(scan_step, entering, entries)
    lower_mask = jnp.tril(jnp.ones((BLOCK, BLOCK), dtype=bool))
    decays = jnp.where(
        lower_mask,
        cumulative[..., :, None] - cumulative[..., None, :] + gate_blocks[..., None, :],
        NEGATIVE,
    )
    carried_log = cumulative + stable_in.T[..., None]
    row_max = jnp.maximum(carried_log, jnp.max(decays, axis=-1))
    within = jnp.where(lower_mask, jnp.exp(decays - row_max[..., None]), 0.0)
    outside = jnp.exp(carried_log - row_max)
    scores = within * jnp.einsum("hctd,hcsd->hcts", query_blocks, key_blocks, precision=highest)
    numerator = outside[..., None] * jnp.einsum(
        "chvk,hctk->hctv", memory_in, query_blocks, precision=highest
    )
    numerator = numerator + jnp.einsum("hcts,hcsv->hctv", scores, value_blocks, precision=highest)
    denominator = outside * jnp.einsum(
        "chk,hctk->hct", normal_in, query_blocks, precision=highest
    ) + jnp.sum(scores, axis=-1)
    result = numerator / jnp.maximum(jnp.abs(denominator), 1.0)[..., None]
    return (
        result.transpose(1, 2, 0, 3)
        .reshape(token_count, head_count * head_width)
        .astype(jnp.bfloat16)
    )


def combine_states(earlier, later_part):
    memory, normal, stable, decay_sum = earlier
    later_memory, later_normal, later_stable, later_decay = later_part
    new_stable = jnp.maximum(later_decay + stable, later_stable)
    former = jnp.exp(later_decay + stable - new_stable)
    latter = jnp.exp(later_stable - new_stable)
    return (
        former[:, None, None] * memory + latter[:, None, None] * later_memory,
        former[:, None] * normal + latter[:, None] * later_normal,
        new_stable,
        decay_sum + later_decay,
    )


def summarize(key_heads, values, gate_in, log_forget):
    head_width = key_heads.shape[-1]
    highest = lax.Precision.HIGHEST
    key_floats = key_heads.astype(jnp.float32) * head_width ** (-0.5)
    cumulative = jnp.cumsum(log_forget, axis=0)
    span_decay = cumulative[-1]
    toward_end = span_decay[None, :] - cumulative + gate_in
    span_max = jnp.max(toward_end, axis=0)
    end_weights = jnp.exp(toward_end - span_max[None, :])
    memory = jnp.einsum(
        "rh,rhv,rhk->hvk", end_weights, values.astype(jnp.float32), key_floats, precision=highest
    )
    normal = jnp.einsum("rh,rhk->hk", end_weights, key_floats, precision=highest)
    return (memory, normal, span_max, span_decay)


def attend(carried, arriving, query_first, query_second, query_positions):
    key_first = arriving[..., :DD]
    key_second = arriving[..., DD : 2 * DD]
    value_part = arriving[..., 2 * DD :]
    key_positions = jnp.arange(arriving.shape[0], dtype=jnp.int32)
    visible = (key_positions[None, :] <= query_positions[:, None]) & (key_positions[None, :] >= 0)
    score_scale = DD ** (-0.5)
    results = []
    for side_index, (query_side, key_side) in enumerate(
        ((query_first, key_first), (query_second, key_second))
    ):
        row_max, totals, accumulated = carried[3 * side_index : 3 * side_index + 3]
        scores = (
            jnp.einsum("qhd,khd->hqk", query_side, key_side, preferred_element_type=jnp.float32)
            * score_scale
        )
        scores = jnp.where(visible[None], scores, NEGATIVE)
        new_max = jnp.maximum(row_max, jnp.max(scores, axis=2))
        weights = jnp.where(visible[None], jnp.exp(scores - new_max[..., None]), 0.0)
        totals = jnp.sum(weights, axis=2)
        accumulated = jnp.einsum(
            "hqk,khd->hqd",
            weights.astype(jnp.bfloat16),
            value_part,
            preferred_element_type=jnp.float32,
        )
        results.extend([new_max, totals, accumulated])
    return tuple(results)


def per_device(
    inputs,
    norm_gain,
    query_weight,
    key_weight,
    value_weight,
    memory_query_weight,
    memory_key_weight,
    memory_value_weight,
    input_gate_weight,
    forget_gate_weight,
    forget_bias,
    decay_shift,
    lambdas,
    head_gain,
    out_weight_attention,
    out_weight_memory,
):
    row_count = inputs.shape[0]
    weights = (
        query_weight,
        key_weight,
        value_weight,
        memory_query_weight,
        memory_key_weight,
        memory_value_weight,
        input_gate_weight,
        forget_gate_weight,
    )
    floats = gather_directly(inputs, "tp", 1).astype(jnp.float32)
    scaled = (floats * norm_gain[None, :]).astype(jnp.bfloat16)
    running_sums = tuple(
        (jnp.dot(scaled, weight, preferred_element_type=jnp.float32) for weight in weights)
    )
    running_sums, squares = (running_sums, jnp.sum(floats * floats, axis=1))
    inverse_rms = lax.rsqrt(squares / norm_gain.shape[0] + EPSILON)[:, None]
    projected = [running * inverse_rms for running in running_sums]

    def split_heads(flat_values):
        return flat_values.astype(jnp.bfloat16).reshape(row_count, -1, HEAD)

    queries = split_heads(projected[0])
    key_heads = split_heads(projected[1])
    values = split_heads(projected[2])
    offset = lax.axis_index(SP) * row_count
    positions = offset + jnp.arange(row_count, dtype=jnp.int32)
    query_first = rotate(queries[..., :DD], positions)
    query_second = rotate(queries[..., DD:], positions)
    packed = jnp.concatenate(
        [rotate(key_heads[..., :DD], positions), rotate(key_heads[..., DD:], positions), values],
        axis=-1,
    )
    head_count = queries.shape[1]
    empty_max = jnp.full((head_count, row_count), NEGATIVE, jnp.float32)
    empty_total = jnp.zeros((head_count, row_count), jnp.float32)
    empty_sums = jnp.zeros((head_count, row_count, HEAD), jnp.float32)
    starting = (empty_max, empty_total, empty_sums, empty_max, empty_total, empty_sums)
    gathered = attend(starting, gather_axes(packed, SP, 0), query_first, query_second, positions)
    first_max, first_total, first_sums, second_max, second_total, second_sums = gathered
    stacked = first_sums / first_total[..., None] - lambdas[:, None, None] * (
        second_sums / second_total[..., None]
    )
    stacked = stacked.transpose(1, 0, 2)
    norm_scale = lax.rsqrt(jnp.mean(stacked * stacked, axis=-1, keepdims=True) + EPSILON)
    attended = (stacked * norm_scale * head_gain).astype(jnp.bfloat16).reshape(row_count, -1)
    gate_in = projected[6]
    log_forget = jax.nn.log_sigmoid(projected[7] + forget_bias[None, :]) + decay_shift
    memory_queries = split_heads(projected[3])
    memory_keys = split_heads(projected[4])
    memory_values = split_heads(projected[5])
    summary = summarize(memory_keys, memory_values, gate_in, log_forget)
    memory_heads = gate_in.shape[1]
    identity = (
        jnp.zeros((memory_heads, HEAD, HEAD), jnp.float32),
        jnp.zeros((memory_heads, HEAD), jnp.float32),
        jnp.full((memory_heads,), NEGATIVE, jnp.float32),
        jnp.zeros((memory_heads,), jnp.float32),
    )
    prefix = carried_in(summary, SP, combine_states, identity)
    start_state = (
        jnp.zeros((memory_heads, HEAD, HEAD), jnp.float32),
        jnp.zeros((memory_heads, HEAD), jnp.float32),
        jnp.zeros((memory_heads,), jnp.float32),
        jnp.zeros((memory_heads,), jnp.float32),
    )
    entering = combine_states(start_state, prefix)[:3]
    memory = memory_blocks(
        memory_queries, memory_keys, memory_values, gate_in, log_forget, entering
    )
    partial_term = jnp.dot(attended, out_weight_attention, preferred_element_type=jnp.float32)
    partial_term = partial_term + jnp.dot(
        memory, out_weight_memory, preferred_element_type=jnp.float32
    )
    return sum_at_owner(partial_term.astype(jnp.bfloat16), "tp", 1).astype(jnp.bfloat16)


def solution(mesh):
    split = Mesh(mesh.devices.reshape(8, 4, mesh.shape["tp"]), ("sp_0", "sp_1", "tp"))
    placed = (
        P(SP, "tp"),
        P(),
        P(None, "tp"),
        P(None, "tp"),
        P(None, "tp"),
        P(None, "tp"),
        P(None, "tp"),
        P(None, "tp"),
        P(None, "tp"),
        P(None, "tp"),
        P("tp"),
        P(SP, "tp"),
        P("tp"),
        P(),
        P("tp", None),
        P("tp", None),
    )
    return jax.shard_map(
        per_device, mesh=split, in_specs=placed, out_specs=P(SP, "tp"), check_vma=False
    )
```

profile of v0, /device:TPU:1, one launch (start us, length us, event | category | flops | bytes accessed | tf_op | source)
XLA Modules:
  0.0 313.6 jit_solution(13800491743508091389)
XLA Ops:
  7.7 1.3 broadcast_in_dim.101
  9.0 6.8 %all-to-all-start = ((bf16[8,384,256]{1,2,0:T(8,128)(2,1)}), bf16[8,384,256]{1,2,0:T(8,128)(2,1)S(1)}, u32[]{:S(2)}, u32[]{:S(2)}) async-start(bf16[8,384,256]{1,2,0:T(8,128)(2,1)} %broadcast_in_dim.101), calls=%async_computation | async-start | bytes 3145728 | tf_op jit(solution)/shard_map/all_to_all | solution.py:26
  15.8 5.0 %iota_compare_fusion = pred[384,12288]{1,0:T(8,128)(4,1)} fusion(s32[384]{0:T(512)S(1)} %iota_add_fusion), kind=kLoop, calls=%fused_computation.26 | loop fusion | flops 4718592 | bytes 4720128 | tf_op jit(solution)/shard_map/le | solution.py:214
  21.6 14.8 %all-to-all-done = bf16[8,384,256]{1,2,0:T(8,128)(2,1)S(1)} async-done(((bf16[8,384,256]{1,2,0:T(8,128)(2,1)}), bf16[8,384,256]{1,2,0:T(8,128)(2,1)S(1)}, u32[]{:S(2)}, u32[]{:S(2)}) %all-to-all-start) | async-done | bytes 1572896 | tf_op jit(solution)/shard_map/all_to_all | solution.py:26
  37.6 1.8 fusion.20
  42.8 1.5 fusion.42
  44.4 2.2 fusion.43
  46.5 1.5 fusion.46
  48.1 1.5 fusion.48
  50.9 1.6 broadcast_in_dim.106
  52.5 10.3 %all-to-all-start.1 = ((f32[32,132,64]{1,2,0:T(8,128)}), f32[32,132,64]{1,2,0:T(8,128)S(1)}, u32[]{:S(2)}, u32[]{:S(2)}) async-start(f32[32,132,64]{1,2,0:T(8,128)} %broadcast_in_dim.106), calls=%async_computation.1 | async-start | bytes 4194304 | tf_op jit(solution)/shard_map/all_to_all | solution.py:26
  66.5 1.5 constant_dynamic-update-slice_fusion.1
  68.0 22.1 %all_gather.6 = bf16[1536,2,128]{0,2,1:T(8,128)(2,1)} all-gather(bf16[384,2,128]{0,2,1:T(8,128)(2,1)} %constant_dynamic-update-slice_fusion.1), channel_id=1, replica_groups=mesh['sp_0'=8,'sp_1'=4,'tp'=8] {'sp_1'}, dimensions={0}, use_global_device_ids=true | all-gather | bytes 983040 | tf_op jit(solution)/shard_map/all_gather | solution.py:38
  91.2 2.1 fusion.41
  94.4 1.9 fusion.71
  96.3 17.2 %all-to-all-done.1 = f32[32,132,64]{1,2,0:T(8,128)S(1)} async-done(((f32[32,132,64]{1,2,0:T(8,128)}), f32[32,132,64]{1,2,0:T(8,128)S(1)}, u32[]{:S(2)}, u32[]{:S(2)}) %all-to-all-start.1) | async-done | bytes 1081376 | tf_op jit(solution)/shard_map/all_to_all | solution.py:26
  113.5 2.0 fusion.126
  115.5 1.6 copy.139
  117.1 1.6 copy.140
  120.9 3.2 %copy.133 = f32[32,128,64]{2,1,0:T(8,128)} copy(f32[32,128,64]{1,2,0:T(8,128)} %slice.289) | data formatting | bytes 2097152 | tf_op jit(solution)/shard_map/reshape;reshape | solution.py:53
  124.1 3.1 %broadcast_select_fusion = f32[32,2,64,64]{3,2,1,0:T(8,128)} fusion(f32[32,2,64,64]{3,2,1,0:T(8,128)} %bitcast.217, pred[32]{0:T(512)(128)(4,1)S(1)} %copy-done.18), kind=kLoop, calls=%fused_computation.74 | loop fusion | flops 262144 | bytes 2097184 | tf_op jit(solution)/shard_map/jit(_where)/select_n | solution.py:72
  128.3 1.7 copy.141
  130.6 1.8 multiply_add_fusion
  132.8 13.3 %while.20 = (s32[]{:T(128)}, f32[2,64,64]{2,1,0:T(8,128)S(1)}, f32[2,64]{1,0:T(2,128)S(1)}, f32[2]{0:T(128)S(1)}, f32[6,2,64,64]{3,2,0,1:T(8,128)}, /*index=5*/f...) while((s32[]{:T(128)}, f32[2,64,64]{2,1,0:T(8,128)S(1)}, ...), condition=%wide.region_12.13_spmd, body=%wide.region_11.12_spmd.sunk | while | flops 24970 | bytes 200465 | solution.py:152
  147.1 1.5 fusion.27
  149.5 21.5 %all-gather.2.cloned.1.call-done = bf16[12288,2,128]{0,2,1:T(8,128)(2,1)} async-done(((bf16[1536,2,128]{0,2,1:T(8,128)(2,1)}), bf16[12288,2,128]{0,2,1:T(8,128)(2,1)}) %all-gather.2.cloned.1.call-update) | async-done | bytes 6291472 | tf_op jit(solution)/shard_map/all_gather | solution.py:38
  171.0 15.3 %fusion.25 = f32[2,384,12288]{2,1,0:T(8,128)} fusion(bf16[12288,2,128]{0,2,1:T(8,128)(2,1)} %all-gather.2.cloned.1.call-done, bf16[384,2,16]{0,2,1:T(8,128)(2,1)S(1)} %copy-done.7, bf16[384,2,16]{0,2,1:T(8,128)(2,1)S(1)} %copy-done.8), kind=kOutput, calls=%fused_computation.40 | convolution fusion | flops 604078080 | bytes 39370752 | tf_op jit(solution)/shard_map/qhd,khd->hqk/dot_general | solution.py:222
  186.3 32.1 %fusion.9 = (f32[2,384]{1,0:T(2,128)S(1)}, f32[2,384]{1,0:T(2,128)S(1)}, f32[2,384,12288]{2,1,0:T(8,128)}) fusion(pred[384,12288]{1,0:T(8,128)(4,1)} %iota_compare_fusion, f32[2,384,12288]{2,1,0:T(8,128)} %fusion.25, bf16[12288,2,128]{0,2,1:T(8,128)(2,1)} %all-gather.2.cloned.1.call-done, bf16[384,2,16]{0,2,1:T(8,128)(2,1)S(1)} %copy-done.10, ...), kind=kOutput, calls=%fused_computation.21 | convolution fusion | flops 660699648 | bytes 81844224 | tf_op jit(solution)/shard_map/qhd,khd->hqk/dot_general | solution.py:222
  218.4 26.7 %fusion.12 = (f32[2,384]{1,0:T(2,128)S(1)}, f32[2,384]{1,0:T(2,128)S(1)}) fusion(f32[2,384,12288]{2,1,0:T(8,128)} %get-tuple-element.192, f32[2,384]{1,0:T(2,128)S(1)} %get-tuple-element.199, pred[384,12288]{1,0:T(8,128)(4,1)} %iota_compare_fusion, f32[2,384]{1,0:T(2,128)S(1)} %get-tuple-element.200, f32[2,384,12288]{2,1,0:T(8,128)} %fusion.25), kind=kLoop, calls=%fused_computation.24 | loop fusion | flops 94370304 | bytes 80228352 | tf_op jit(solution)/shard_map/reduce_sum | solution.py:228
  245.1 17.8 %fusion.66 = f32[384,2,64]{0,2,1:T(8,128)S(1)} fusion(bf16[12288,2,128]{0,2,1:T(8,128)(2,1)} %all-gather.2.cloned.1.call-done, f32[2,384,12288]{2,1,0:T(8,128)} %fusion.25, f32[2,384]{1,0:T(2,128)S(1)} %get-tuple-element.200, pred[384,12288]{1,0:T(8,128)(4,1)} %iota_compare_fusion, f32[384,2]{0,1:T(2,128)S(1)} %bitcast.249), kind=kOutput, calls=%fused_computation.72 | convolution fusion | flops 1255194624 | bytes 45815808 | tf_op jit(solution)/shard_map/hqk,khd->hqd/dot_general | solution.py:229
  263.0 18.0 %multiply_reduce_fusion.1 = (f32[384,2]{0,1:T(2,128)S(1)}, f32[384,2,64]{0,2,1:T(8,128)S(1)}) fusion(f32[384,2,64]{0,2,1:T(8,128)S(1)} %fusion.66, f32[384,2]{0,1:T(2,128)S(1)} %bitcast.248, bf16[12288,2,128]{0,2,1:T(8,128)(2,1)} %all-gather.2.cloned.1.call-done, f32[2,384,12288]{2,1,0:T(8,128)} %get-tuple-element.192, ...), kind=kOutput, calls=%fused_computation.90 | convolution fusion | flops 1255390464 | bytes 46015496 | tf_op jit(solution)/shard_map/hqk,khd->hqd/dot_general | solution.py:229
  282.4 23.5 %all_to_all.15 = bf16[8,384,256]{2,1,0:T(8,128)(2,1)S(1)} all-to-all(bf16[8,384,256]{2,1,0:T(8,128)(2,1)S(1)} %bitcast.218), channel_id=1, replica_groups=mesh['sp_0'=8,'sp_1'=4,'tp'=8] {'tp'}, dimensions={0} | all-to-all | bytes 3145728 | tf_op jit(solution)/shard_map/all_to_all | solution.py:88
  (207 shorter events, 35.2 us)
Async XLA Ops:
  6.5 274.5 %copy-start = (bf16[128,2048]{1,0:T(8,128)(2,1)S(1)}, bf16[128,2048]{1,0:T(8,128)(2,1)}, u32[]{:S(2)}) copy-start(bf16[128,2048]{1,0:T(8,128)(2,1)} %param.32) | copy-start | bytes 1572868
  6.5 31.0 %copy-start.15 = (f32[2048]{0:T(1024)S(1)}, f32[2048]{0:T(1024)}, u32[]{:S(2)}) copy-start(f32[2048]{0:T(1024)} %param.19) | copy-start | bytes 24580
  9.0 30.4 %copy-start.16 = (bf16[2048,2]{0,1:T(2,128)(2,1)S(1)}, bf16[2048,2]{0,1:T(2,128)(2,1)}, u32[]{:S(2)}) copy-start(bf16[2048,2]{0,1:T(2,128)(2,1)} %param.27) | copy-start | bytes 24580
  9.0 30.4 %copy-start.19 = (f32[384,2]{0,1:T(2,128)S(1)}, f32[384,2]{0,1:T(2,128)}, u32[]{:S(2)}) copy-start(f32[384,2]{0,1:T(2,128)} %param.29) | copy-start | bytes 9220
  9.0 30.4 %copy-start.20 = (f32[2]{0:T(128)S(1)}, f32[2]{0:T(128)}, u32[]{:S(2)}) copy-start(f32[2]{0:T(128)} %param.28) | copy-start | bytes 28
  9.0 27.4 %all-to-all-start = ((bf16[8,384,256]{1,2,0:T(8,128)(2,1)}), bf16[8,384,256]{1,2,0:T(8,128)(2,1)S(1)}, u32[]{:S(2)}, u32[]{:S(2)}) async-start(bf16[8,384,256]{1,2,0:T(8,128)(2,1)} %broadcast_in_dim.101), calls=%async_computation | async-start | bytes 3145728 | tf_op jit(solution)/shard_map/all_to_all | solution.py:26
  15.8 25.2 %copy-start.17 = (bf16[2048,2]{0,1:T(2,128)(2,1)S(1)}, bf16[2048,2]{0,1:T(2,128)(2,1)}, u32[]{:S(2)}) copy-start(bf16[2048,2]{0,1:T(2,128)(2,1)} %param.26) | copy-start | bytes 24580
  15.8 26.5 %copy-start.22 = (bf16[2048,128]{1,0:T(8,128)(2,1)S(1)}, bf16[2048,128]{1,0:T(8,128)(2,1)}, u32[]{:S(2)}) copy-start(bf16[2048,128]{1,0:T(8,128)(2,1)} %param.25) | copy-start | bytes 1572868
  36.4 1.1 copy-start.2
  37.6 10.5 %copy-start.11 = (f32[384]{0:T(512)}, f32[384]{0:T(512)S(1)}, u32[]{:S(2)}) copy-start(f32[384]{0:T(512)S(1)} %add_rsqrt_fusion.1) | copy-start | bytes 4612
  39.4 8.7 %copy-start.1 = (bf16[384,2048]{0,1:T(8,128)(2,1)}, bf16[384,2048]{0,1:T(8,128)(2,1)S(1)}, u32[]{:S(2)}) copy-start(bf16[384,2048]{0,1:T(8,128)(2,1)S(1)} %fusion.20) | copy-start | bytes 4718596
  42.3 21.3 %copy-start.13 = (f32[2,6]{1,0:T(2,128)}, f32[2,6]{1,0:T(2,128)S(1)}, u32[]{:S(2)}) copy-start(f32[2,6]{1,0:T(2,128)S(1)} %slice_reduce_fusion) | copy-start | bytes 148
  50.9 1.6 copy-start.6
  52.5 61.0 %all-to-all-start.1 = ((f32[32,132,64]{1,2,0:T(8,128)}), f32[32,132,64]{1,2,0:T(8,128)S(1)}, u32[]{:S(2)}, u32[]{:S(2)}) async-start(f32[32,132,64]{1,2,0:T(8,128)} %broadcast_in_dim.106), calls=%async_computation.1 | async-start | bytes 4194304 | tf_op jit(solution)/shard_map/all_to_all | solution.py:26
  62.8 108.3 %all-gather.2.cloned.1.call-start = ((), (), s32[]{:S(2)}) async-start(), calls=%async_computation.3 | async-start | bytes 7077888 | tf_op jit(solution)/shard_map/all_gather | solution.py:38
  63.0 27.2 %copy-start.14 = (f32[2,6]{1,0:T(2,128)}, f32[2,6]{1,0:T(2,128)S(1)}, u32[]{:S(2)}) copy-start(f32[2,6]{1,0:T(2,128)S(1)} %fusion.106) | copy-start | bytes 148
  94.4 29.7 %copy-start.18 = (pred[32]{0:T(512)(128)(4,1)S(1)}, pred[32]{0:T(512)(128)(4,1)}, u32[]{:S(2)}) copy-start(pred[32]{0:T(512)(128)(4,1)} %iota_compare_fusion.2) | copy-start | bytes 100
  124.1 8.7 %copy-start.12 = (f32[6,2]{1,0:T(8,128)S(1)}, f32[6,2]{1,0:T(8,128)}, u32[]{:S(2)}) copy-start(f32[6,2]{1,0:T(8,128)} %custom-call.3) | copy-start | bytes 148
  124.1 8.7 %copy-start.23 = (f32[6,2,64]{2,1,0:T(2,128)S(1)}, f32[6,2,64]{2,1,0:T(2,128)}, u32[]{:S(2)}) copy-start(f32[6,2,64]{2,1,0:T(2,128)} %custom-call.2) | copy-start | bytes 9220
  128.3 18.0 %copy-start.4 = (bf16[2,6,64,64]{2,3,1,0:T(8,128)(2,1)S(1)}, bf16[2,6,64,64]{2,3,1,0:T(8,128)(2,1)}, u32[]{:S(2)}) copy-start(bf16[2,6,64,64]{2,3,1,0:T(8,128)(2,1)} %copy.131) | copy-start | bytes 294916
  128.3 20.3 %copy-start.3 = (bf16[6,64,2,64]{3,1,0,2:T(8,128)(2,1)S(1)}, bf16[6,64,2,64]{3,1,0,2:T(8,128)(2,1)}, u32[]{:S(2)}) copy-start(bf16[6,64,2,64]{3,1,0,2:T(8,128)(2,1)} %copy.106) | copy-start | bytes 294916
  130.6 40.4 %copy-start.7 = (bf16[384,2,16]{0,2,1:T(8,128)(2,1)S(1)}, bf16[384,2,16]{0,2,1:T(8,128)(2,1)}, u32[]{:S(2)}) copy-start(bf16[384,2,16]{0,2,1:T(8,128)(2,1)} %get-tuple-element.175) | copy-start | bytes 73732
  130.6 40.4 %copy-start.8 = (bf16[384,2,16]{0,2,1:T(8,128)(2,1)S(1)}, bf16[384,2,16]{0,2,1:T(8,128)(2,1)}, u32[]{:S(2)}) copy-start(bf16[384,2,16]{0,2,1:T(8,128)(2,1)} %get-tuple-element.176) | copy-start | bytes 73732
  171.0 15.3 %copy-start.9 = (bf16[384,2,16]{0,2,1:T(8,128)(2,1)S(1)}, bf16[384,2,16]{0,2,1:T(8,128)(2,1)}, u32[]{:S(2)}) copy-start(bf16[384,2,16]{0,2,1:T(8,128)(2,1)} %get-tuple-element.167) | copy-start | bytes 73732
  171.0 15.3 %copy-start.10 = (bf16[384,2,16]{0,2,1:T(8,128)(2,1)S(1)}, bf16[384,2,16]{0,2,1:T(8,128)(2,1)}, u32[]{:S(2)}) copy-start(bf16[384,2,16]{0,2,1:T(8,128)(2,1)} %get-tuple-element.168) | copy-start | bytes 73732
  245.1 17.8 %copy-start.24 = (f32[2]{0:T(128)S(1)}, f32[2]{0:T(128)}, u32[]{:S(2)}) copy-start(f32[2]{0:T(128)} %param.30) | copy-start | bytes 28
  262.9 18.1 %copy-start.21 = (f32[64]{0:T(128)S(1)}, f32[64]{0:T(128)}, u32[]{:S(2)}) copy-start(f32[64]{0:T(128)} %param.31) | copy-start | bytes 772
  262.9 18.7 %copy-start.5 = (bf16[128,2048]{1,0:T(8,128)(2,1)S(1)}, bf16[128,2048]{1,0:T(8,128)(2,1)}, u32[]{:S(2)}) copy-start(bf16[128,2048]{1,0:T(8,128)(2,1)} %param.33) | copy-start | bytes 1572868
Sparse Core Ops, SparseCore 0:
  90.3 80.6 all-gather.1
where the time goes:
time: 315 us; the launch traced here: 314 us
  matrix products  100 us (32%)
  other arithmetic  55.2 us (18%)
  waiting for transfers between devices  53.6 us (17%)
  blocking collectives  45.6 us (14%)
  local copies, waits for them, and re-layouts  28 us (9%)
  starting transfers between devices  17.1 us (5%)
  between operations  14 us (4%)
    dot_general x2, matrix products, attend(): jnp.einsum('qhd,khd->hqk', query_side, key_side, preferred_element_type=j...  47.4 us
    dot_general x2, matrix products, attend(): jnp.einsum('hqk,khd->hqd', weights.astype(jnp.bfloat16), value_part, pref...  35.8 us
    all_to_all x2, waiting for transfers between devices, from_everyone(): lax.all_to_all(jnp.broadcast_to(array[None], (devices, *array.shape)), ax...  32 us
    reduce_sum x1, other arithmetic, attend(): totals = jnp.sum(weights, axis=2)  26.7 us
    all_to_all x1, blocking collectives, sum_at_owner(): lax.all_to_all(pieces, axis, split_axis=0, concat_axis=0, tiled=True)  23.5 us
    all_gather x1, blocking collectives, gather_axes(): filled = lax.all_gather(filled, axes[number], axis=dim, tiled=True)  22.1 us
    all_gather x1, waiting for transfers between devices, gather_axes(): filled = lax.all_gather(filled, axes[number], axis=dim, tiled=True)  21.5 us
    all_to_all x2, starting transfers between devices, from_everyone(): lax.all_to_all(jnp.broadcast_to(array[None], (devices, *array.shape)), ax...  17.1 us
  transfers between devices with their start and end apart: 3, of which 3 were waited for; matrix products, arithmetic and copies ran while one was open for 17% of the time, Pallas kernels for 0%

commit v1 on v0

v1 whole, which is shorter than its diff:
```python
import jax
import jax.numpy as jnp
from jax import lax
from jax.experimental import pallas as pl
from jax.experimental.pallas import tpu as pltpu
from jax.sharding import PartitionSpec as P

HEAD = 64
DD = 32
EPSILON = 1e-06
ROTARY_BASE = 10000.0
NEGATIVE = -1e30
LOG2E = 1.4426950408889634
SPANS = 32
ROUNDS = 5
CHUNKS = 4
MESH = pl.DeviceIdType.MESH
F32 = jnp.float32
BF16 = jnp.bfloat16


def ring_position(ring, span):
    a, b = span // 4, span % 4
    if ring == 0:
        return 4 * a + (a + b) % 4
    r = (a + 5 * b) % 8
    return 4 * (b + 4 * (r // 4)) + r % 4


def span_on_ring(ring, position):
    u, r = position // 4, position % 4
    if ring == 0:
        return 4 * u + (r + 32 - u) % 4
    return 4 * ((3 * u + r) % 8) + u % 4


def dot(a, b):
    return jnp.dot(a, b, preferred_element_type=F32)


def dot_t(a, b):
    return lax.dot_general(a, b, (((1,), (1,)), ((), ())), preferred_element_type=F32)


def halves(a):
    high = a.astype(BF16)
    return high, (a - high.astype(F32)).astype(BF16)


def thirds(a):
    high = a.astype(BF16)
    rest = a - high.astype(F32)
    middle = rest.astype(BF16)
    return high, middle, (rest - middle.astype(F32)).astype(BF16)


def layer_kernel(
    x, gain, cosine, sine, wq, wk, wv, wmq, wmk, wmv, wig, wfg, bias, decay, lambdas, head_gain,
    woa, wom, out,
    xg, xs, squares, w, wi, wf, wo, held, qs, mq, mk, mv, gates, acc, top, st_in, st_out, st_before,
    num_local, log_local, cat, to_partner, from_partner, to_ring, from_ring,
    load_sem, gather_send, gather_recv, ring_send, ring_recv, scan_send, scan_recv,
    pair_send, pair_recv, sum_send, sum_recv,
):
    rows = x.shape[0]
    half_rows = rows // 2
    chunk = rows // CHUNKS
    sp = lax.axis_index("sp")
    tp = lax.axis_index("tp")
    y, c = tp // 2, tp % 2
    right = 2 * ((y + 1) % 4) + c
    left = 2 * ((y + 3) % 4) + c
    across = 2 * ((y + 2) % 4) + c
    partner = 2 * y + 1 - c
    t0, t1 = ring_position(0, sp), ring_position(1, sp)
    nexts = [span_on_ring(ring, (t + step) % SPANS)
             for ring, t in ((0, t0), (1, t1)) for step in (1, SPANS - 1)]

    def remote(src, dst, send, recv, span, seat):
        return pltpu.make_async_remote_copy(
            src_ref=src, dst_ref=dst, send_sem=send, recv_sem=recv,
            device_id=(span, seat), device_id_type=MESH)

    own_load = pltpu.make_async_copy(x, xg.at[tp], load_sem.at[0])
    own_load.start()
    loads = []
    for number, (weight, tile, at) in enumerate(
            ((wq, 0, 0), (wk, 0, 128), (wv, 1, 0), (wmq, 1, 128), (wmk, 2, 0), (wmv, 2, 128))):
        loads.append(pltpu.make_async_copy(
            weight, w.at[tile, :, pl.ds(at, 128)], load_sem.at[1 + number]))
    loads.append(pltpu.make_async_copy(wig, wi, load_sem.at[7]))
    loads.append(pltpu.make_async_copy(wfg, wf, load_sem.at[8]))
    for load in loads:
        load.start()
    out_loads = []
    for j in range(8):
        for part, weight in enumerate((woa, wom)):
            out_loads.append(pltpu.make_async_copy(
                weight.at[:, pl.ds(256 * j, 256)], wo.at[j, pl.ds(128 * part, 128), :],
                load_sem.at[9 + 2 * j + part]))
    for load in out_loads:
        load.start()

    barrier = pltpu.get_barrier_semaphore()
    greeted = [(sp, right), (sp, left), (sp, partner)] + [(span, tp) for span in nexts]
    for number in range(ROUNDS):
        greeted.append(((sp + 2 ** number) % SPANS, tp))
        if number < ROUNDS - 1:
            greeted.append(((sp + SPANS - 2 ** number) % SPANS, tp))
    for span, seat in greeted:
        pl.semaphore_signal(barrier, inc=1, device_id=(span, seat), device_id_type=MESH)
    pl.semaphore_wait(barrier, len(greeted))

    def piece(seat, half):
        return xg.at[seat, pl.ds(half * half_rows, half_rows), :]

    def gather(number, ref, seat):
        return remote(ref, ref, gather_send.at[number], gather_recv.at[number], sp, seat)

    sends = {
        0: gather(0, piece(tp, 0), right),
        1: gather(1, piece(tp, 1), right),
        2: gather(2, piece(tp, 1), left),
        3: gather(3, piece(tp, 0), left),
        4: gather(4, xg.at[tp], partner),
        5: gather(5, piece(left, 0), right),
        6: gather(6, piece(left, 0), partner),
        7: gather(7, piece(right, 1), left),
        8: gather(8, piece(right, 1), partner),
        9: gather(9, piece(left, 1), partner),
        10: gather(10, piece(right, 0), partner),
        11: gather(11, piece(across, 0), partner),
        12: gather(12, piece(across, 1), partner),
    }
    own_load.wait()
    for number in (0, 2, 1, 3, 4):
        sends[number].start()

    def absorb(seat):
        block = xg[seat].astype(F32)
        squares[...] += block * block
        xs[seat] = (block * gain[seat]).astype(BF16)

    squares[...] = jnp.zeros_like(squares)
    absorb(tp)
    sends[0].wait_recv()
    sends[5].start()
    sends[6].start()
    sends[2].wait_recv()
    sends[7].start()
    sends[8].start()
    sends[4].wait_recv()
    absorb(partner)
    sends[1].wait_recv()
    sends[9].start()
    sends[3].wait_recv()
    sends[10].start()
    absorb(left)
    absorb(right)
    sends[5].wait_recv()
    sends[11].start()
    sends[7].wait_recv()
    sends[12].start()
    for number in (6, 8, 9, 10):
        sends[number].wait_recv()
    absorb(2 * ((y + 1) % 4) + 1 - c)
    absorb(2 * ((y + 3) % 4) + 1 - c)
    absorb(across)
    sends[11].wait_recv()
    sends[12].wait_recv()
    absorb(2 * ((y + 2) % 4) + 1 - c)
    for number in range(13):
        sends[number].wait_send()
    for load in loads:
        load.wait()

    inverse = lax.rsqrt(
        jnp.sum(squares[...], axis=1, keepdims=True) * (1.0 / 2048.0) + EPSILON)
    scaled = jnp.concatenate([xs[j] for j in range(8)], axis=1)
    lane = lax.broadcasted_iota(jnp.int32, (rows, 128), 1)
    low = lane < HEAD
    former = lane % 32 < 16

    def rotated(flat):
        floats = flat.astype(BF16).astype(F32)
        swapped = jnp.where(former, pltpu.roll(floats, 112, 1), pltpu.roll(floats, 16, 1))
        return (floats * cosine[...] + swapped * sine[...]).astype(BF16).astype(F32)

    product = dot(scaled, w[0]) * inverse
    queries = rotated(product[:, :128])
    keys = rotated(product[:, 128:])
    product = dot(scaled, w[1]) * inverse
    values = product[:, :128].astype(BF16).astype(F32)
    mq[...] = product[:, 128:].astype(BF16)
    held[0, t0] = jnp.where(low, keys, pltpu.roll(values, 64, 1)).astype(BF16)
    held[1, t1] = jnp.where(low, pltpu.roll(keys, 64, 1), values).astype(BF16)
    for head in range(2):
        turned = queries if head == 0 else pltpu.roll(queries, 64, 1)
        for side in range(2):
            inside = (lane >= DD * side) & (lane < DD * side + DD)
            qs[head, side * rows:(side + 1) * rows, :] = jnp.where(inside, turned, 0.0).astype(BF16)

    def passing(stream, step, number):
        ring, way = stream // 2, stream % 2
        t = (t0, t1)[ring]
        origin = (t + SPANS - step) % SPANS if way == 0 else (t + step) % SPANS
        ref = held.at[ring, origin, pl.ds(number * chunk, chunk), :]
        return remote(ref, ref, ring_send.at[stream, number],
                      ring_recv.at[stream, step, number], nexts[stream], tp)

    for number in range(CHUNKS):
        for stream in range(4):
            passing(stream, 0, number).start()

    product = dot(scaled, w[2]) * inverse
    mk[...] = product[:, :128].astype(BF16)
    mv[...] = product[:, 128:].astype(BF16)
    gate_in = dot(scaled, wi[...]) * inverse
    forget = dot(scaled, wf[...]) * inverse

    def log_sigmoid(a):
        return jnp.minimum(a, 0.0) - jnp.log1p(jnp.exp(-jnp.abs(a)))

    def per_head(parts):
        return jnp.where(low, parts[0], parts[1])

    log_forget = per_head([
        log_sigmoid(forget[:, h:h + 1] + bias[h]) + decay[:, h:h + 1] for h in range(2)])
    gate = per_head([gate_in[:, h:h + 1] for h in range(2)])
    before_or_at = (lax.broadcasted_iota(jnp.int32, (rows, rows), 1)
                    <= lax.broadcasted_iota(jnp.int32, (rows, rows), 0))
    triangle = jnp.where(before_or_at, 1.0, 0.0).astype(BF16)
    high, middle, small = thirds(log_forget)
    cumulative = dot(triangle, high) + dot(triangle, middle) + dot(triangle, small)
    gates[0] = cumulative
    gates[1] = gate - cumulative
    span_decay = cumulative[rows - 1:rows, :]
    toward_end = span_decay + gates[1]
    span_top = jnp.max(toward_end, axis=0, keepdims=True)
    end_weights = jnp.exp(toward_end - span_top)
    key_floats = mk[...].astype(F32) * 0.125
    weighted = jnp.transpose(end_weights * mv[...].astype(F32))
    high, small = halves(weighted)
    keys_exact = key_floats.astype(BF16)
    outer = dot(high, keys_exact) + dot(small, keys_exact)
    row = lax.broadcasted_iota(jnp.int32, (8, 128), 0)

    def tail(normal, stable, decays):
        return jnp.where(row == 0, normal, jnp.where(row == 1, stable, decays))

    low_square = low[:HEAD]
    st_out[0, 0:HEAD, :] = jnp.where(low_square, outer[:HEAD], outer[HEAD:])
    st_out[0, HEAD:HEAD + 8, :] = tail(
        jnp.sum(end_weights * key_floats, axis=0, keepdims=True), span_top, span_decay)
    st_before[0:HEAD, :] = jnp.zeros((HEAD, 128), F32)
    st_before[HEAD:HEAD + 8, :] = tail(0.0, NEGATIVE, 0.0) + jnp.zeros((8, 128), F32)

    def scan_copy(number):
        target = (sp + lax.shift_left(jnp.int32(1), jnp.int32(number))) % SPANS
        return remote(st_out.at[number], st_in.at[number], scan_send.at[number],
                      scan_recv.at[number], target, tp)

    def joined(earlier, later):
        old, new = earlier[1], later[1]
        decays, stable, later_stable = new[2:3], old[1:2], new[1:2]
        highest = jnp.maximum(decays + stable, later_stable)
        first = jnp.exp(decays + stable - highest)
        second = jnp.exp(later_stable - highest)
        return (first * earlier[0] + second * later[0],
                tail(first * old[0:1] + second * new[0:1], highest, old[2:3] + decays))

    scale = DD ** (-0.5) * LOG2E
    ones_low = low

    def visit(ring, position, mask=None):
        block = held[ring, position]
        extended = jnp.where(ones_low, jnp.ones_like(block), block)
        scores = dot_t(qs[ring], block)
        if mask is not None:
            scores = jnp.where(mask, scores, NEGATIVE)
            highest = jnp.broadcast_to(jnp.max(scores, axis=1, keepdims=True), (2 * rows, 128))
        else:
            old = top[ring]
            highest = jnp.maximum(old, jnp.max(scores, axis=1, keepdims=True))
        shift = highest * scale
        weights = jnp.exp2(scores * scale - jnp.concatenate([shift] * (rows // 128), axis=1))
        product = dot(weights.astype(BF16), extended)
        if mask is not None:
            acc[ring] = product
        else:
            acc[ring] = acc[ring] * jnp.exp2((old - highest) * scale) + product
        top[ring] = highest

    causal = jnp.concatenate([before_or_at, before_or_at], axis=0)
    visit(0, t0, causal)
    scan_copy(0).start()
    visit(1, t1, causal)

    def local_memory():
        sums, tops, totals = [], [], []
        turned = jnp.transpose(gates[1])
        for head in range(2):
            inside = low if head == 0 else ~low
            gap = gates[0][:, HEAD * head:HEAD * head + 1] + turned[HEAD * head:HEAD * head + 1, :]
            gap = jnp.where(before_or_at, gap, NEGATIVE)
            highest = jnp.max(gap, axis=1, keepdims=True)
            within = jnp.exp(gap - highest)
            mine = jnp.where(inside, mq[...].astype(F32), 0.0).astype(BF16)
            scores = within * (dot_t(mine, mk[...]) * 0.125)
            high, small = halves(scores)
            sums.append(dot(high, mv[...]) + dot(small, mv[...]))
            totals.append(jnp.sum(scores, axis=1, keepdims=True))
            tops.append(highest)
        num_local[0] = per_head(sums)
        num_local[1] = per_head(totals) + jnp.zeros((rows, 128), F32)
        log_local[...] = per_head(tops) + jnp.zeros((rows, 128), F32)

    def scan_round(number):
        scan_copy(number).wait_recv()
        memory = st_in[number, 0:HEAD, :]
        ending = st_in[number, HEAD:HEAD + 8, :]

        @pl.when(sp >= lax.shift_left(jnp.int32(1), jnp.int32(number)))
        def _():
            done = joined((memory, ending), (st_before[0:HEAD, :], st_before[HEAD:HEAD + 8, :]))
            st_before[0:HEAD, :] = done[0]
            st_before[HEAD:HEAD + 8, :] = done[1]

        @pl.when(number < ROUNDS - 1)
        def _():
            mine = (st_out[number, 0:HEAD, :], st_out[number, HEAD:HEAD + 8, :])
            whole = joined((memory, ending), mine)
            reached = sp >= lax.shift_left(jnp.int32(1), jnp.int32(number))
            st_out[number + 1, 0:HEAD, :] = jnp.where(reached, whole[0], mine[0])
            st_out[number + 1, HEAD:HEAD + 8, :] = jnp.where(reached, whole[1], mine[1])

    def step_body(step, unused):
        def sub_step(number, unused):
            for stream in range(4):
                if stream % 2 == 0:
                    passing(stream, step - 1, number).wait_recv()

                    @pl.when(step < 16)
                    def _():
                        passing(stream, step - 1, number).wait_send()
                        passing(stream, step, number).start()
                else:
                    @pl.when(step < 16)
                    def _():
                        passing(stream, step - 1, number).wait_recv()

                    @pl.when(step < 15)
                    def _():
                        passing(stream, step - 1, number).wait_send()
                        passing(stream, step, number).start()
            if CHUNKS == 4:
                attend_stream(step - 1, number)
            else:
                for k in range(4 // CHUNKS):
                    attend_stream(step - 1, number * (4 // CHUNKS) + k)
            return unused

        lax.fori_loop(0, CHUNKS, sub_step, 0)

        @pl.when(step == 1)
        def _():
            local_memory()

        @pl.when((step % 3 == 2) & (step < 15))
        def _():
            scan_round(step // 3)

        @pl.when((step % 3 == 0) & (step < 13))
        def _():
            scan_copy(step // 3).start()

        return unused

    def attend_stream(step, stream):
        ring, way = stream // 2, stream % 2
        start = t0 + ring * (t1 - t0)
        position = (start + way * (2 * step) + SPANS - step) % SPANS
        first, second = span_on_ring(0, position), span_on_ring(1, position)
        origin = first + ring * (second - first)

        @pl.when(origin < sp)
        def _():
            visit(ring, position)

    lax.fori_loop(1, 17, step_body, 0)
    for number in range(CHUNKS):
        for stream in range(4):
            passing(stream, 15 if stream % 2 == 0 else 14, number).wait_send()
    attend_stream(16, 0)
    attend_stream(16, 2)
    for number in range(ROUNDS):
        scan_copy(number).wait_send()

    rooted = []
    for head in range(2):
        sides = []
        for side in range(2):
            part = acc[head, side * rows:(side + 1) * rows, :]
            sides.append(part / pltpu.roll(part, 64, 1))
        difference = sides[0] - lambdas[head] * sides[1]
        squared = jnp.where(low, 0.0, difference * difference)
        mean = jnp.sum(squared, axis=1, keepdims=True) * (1.0 / HEAD)
        rooted.append(difference * lax.rsqrt(mean + EPSILON))
    cat[:, 0:128] = (jnp.where(low, pltpu.roll(rooted[0], 64, 1), rooted[1])
                     * head_gain[...]).astype(BF16)

    start_memory = jnp.zeros((HEAD, 128), F32)
    start_tail = jnp.zeros((8, 128), F32)
    entered = joined((start_memory, start_tail), (st_before[0:HEAD, :], st_before[HEAD:HEAD + 8, :]))
    memory_in, normal_in, stable_in = entered[0], entered[1][0:1], entered[1][1:2]
    spread = jnp.concatenate(
        [jnp.where(low_square, memory_in, 0.0), jnp.where(low_square, 0.0, memory_in)], axis=0)
    spread_normal = jnp.concatenate(
        [jnp.where(low_square, normal_in, 0.0), jnp.where(low_square, 0.0, normal_in)], axis=0)
    carried_log = gates[0] + stable_in
    row_top = jnp.maximum(carried_log, log_local[...])
    outside = jnp.exp(carried_log - row_top)
    inside = jnp.exp(log_local[...] - row_top)
    high, small = halves(spread)
    numerator = outside * (dot_t(mq[...], high) + dot_t(mq[...], small)) + inside * num_local[0]
    high, small = halves(spread_normal)
    denominator = outside * (dot_t(mq[...], high) + dot_t(mq[...], small)) + inside * num_local[1]
    cat[:, 128:256] = (numerator / jnp.maximum(jnp.abs(denominator), 1.0)).astype(BF16)

    for load in out_loads:
        load.wait()
    both = cat[...]

    def share(seat):
        return dot(both, wo[seat]).astype(BF16)

    offsets = (2, 1, 3, 0)
    pairs = []
    for number, offset in enumerate(offsets):
        to_partner[number] = share(2 * ((y + offset) % 4) + 1 - c)
        pairs.append(remote(to_partner.at[number], from_partner.at[number], pair_send.at[number],
                            pair_recv.at[number], sp, partner))
        pairs[number].start()

    def summed(number):
        own = share(2 * ((y + offsets[number]) % 4) + c).astype(F32)
        pairs[number].wait_recv()
        return own + from_partner[number].astype(F32)

    def shift(number, seat):
        return remote(to_ring.at[number], from_ring.at[number], sum_send.at[number],
                      sum_recv.at[number], sp, seat)

    shifts = [shift(0, right), shift(1, left), shift(2, right), shift(3, right), shift(4, left),
              shift(5, left)]
    total = summed(0)
    to_ring[0] = total[:half_rows].astype(BF16)
    to_ring[1] = total[half_rows:].astype(BF16)
    shifts[0].start()
    shifts[1].start()
    total = summed(1)
    to_ring[2] = total[half_rows:].astype(BF16)
    shifts[2].start()
    rest = total[:half_rows]
    total = summed(2)
    to_ring[4] = total[:half_rows].astype(BF16)
    shifts[4].start()
    shifts[0].wait_recv()
    to_ring[3] = (rest + from_ring[0].astype(F32)).astype(BF16)
    shifts[3].start()
    shifts[1].wait_recv()
    to_ring[5] = (total[half_rows:] + from_ring[1].astype(F32)).astype(BF16)
    shifts[5].start()
    total = summed(3)
    for number in (2, 4):
        shifts[number].wait_recv()
    lower = total[half_rows:] + from_ring[2].astype(F32)
    upper = total[:half_rows] + from_ring[4].astype(F32)
    shifts[3].wait_recv()
    shifts[5].wait_recv()
    out[0:half_rows, :] = (upper + from_ring[3].astype(F32)).astype(BF16)
    out[half_rows:rows, :] = (lower + from_ring[5].astype(F32)).astype(BF16)
    for copy in pairs + shifts:
        copy.wait_send()


def per_device(
    inputs, norm_gain, query_weight, key_weight, value_weight, memory_query_weight,
    memory_key_weight, memory_value_weight, input_gate_weight, forget_gate_weight, forget_bias,
    decay_shift, lambdas, head_gain, out_weight_attention, out_weight_memory,
):
    rows, columns = inputs.shape
    positions = (lax.axis_index("sp") * rows + jnp.arange(rows, dtype=jnp.int32)).astype(F32)
    middle = DD // 2
    inverse = 1.0 / ROTARY_BASE ** (jnp.arange(middle, dtype=F32) / middle)
    angles = positions[:, None] * inverse[None, :]
    cosine, sine = jnp.cos(angles), jnp.sin(angles)
    cosine = jnp.concatenate([cosine] * 8, axis=1)
    sine = jnp.concatenate([-sine, sine] * 4, axis=1)
    vmem = pl.BlockSpec(memory_space=pltpu.VMEM)
    smem = pl.BlockSpec(memory_space=pltpu.SMEM)
    anywhere = pl.BlockSpec(memory_space=pl.ANY)
    half = rows // 2
    scratch = [
        pltpu.VMEM((8, rows, columns), BF16),
        pltpu.VMEM((8, rows, columns), BF16),
        pltpu.VMEM((rows, columns), F32),
        pltpu.VMEM((3, 2048, 256), BF16),
        pltpu.VMEM((2048, 2), BF16),
        pltpu.VMEM((2048, 2), BF16),
        pltpu.VMEM((8, 256, 256), BF16),
        pltpu.VMEM((2, SPANS, rows, 128), BF16),
        pltpu.VMEM((2, 2 * rows, 128), BF16),
        pltpu.VMEM((rows, 128), BF16),
        pltpu.VMEM((rows, 128), BF16),
        pltpu.VMEM((rows, 128), BF16),
        pltpu.VMEM((2, rows, 128), F32),
        pltpu.VMEM((2, 2 * rows, 128), F32),
        pltpu.VMEM((2, 2 * rows, 128), F32),
        pltpu.VMEM((ROUNDS, HEAD + 8, 128), F32),
        pltpu.VMEM((ROUNDS, HEAD + 8, 128), F32),
        pltpu.VMEM((HEAD + 8, 128), F32),
        pltpu.VMEM((2, rows, 128), F32),
        pltpu.VMEM((rows, 128), F32),
        pltpu.VMEM((rows, 256), BF16),
        pltpu.VMEM((4, rows, 256), BF16),
        pltpu.VMEM((4, rows, 256), BF16),
        pltpu.VMEM((6, half, 256), BF16),
        pltpu.VMEM((6, half, 256), BF16),
        pltpu.SemaphoreType.DMA((25,)),
        pltpu.SemaphoreType.DMA((13,)),
        pltpu.SemaphoreType.DMA((13,)),
        pltpu.SemaphoreType.DMA((4, CHUNKS)),
        pltpu.SemaphoreType.DMA((4, 16, CHUNKS)),
        pltpu.SemaphoreType.DMA((ROUNDS,)),
        pltpu.SemaphoreType.DMA((ROUNDS,)),
        pltpu.SemaphoreType.DMA((4,)),
        pltpu.SemaphoreType.DMA((4,)),
        pltpu.SemaphoreType.DMA((6,)),
        pltpu.SemaphoreType.DMA((6,)),
    ]
    return pl.pallas_call(
        layer_kernel,
        out_shape=jax.ShapeDtypeStruct((rows, columns), BF16),
        in_specs=[anywhere, vmem, vmem, vmem] + [anywhere] * 8
        + [smem, vmem, smem, vmem, anywhere, anywhere],
        out_specs=vmem,
        scratch_shapes=scratch,
        compiler_params=pltpu.CompilerParams(
            collective_id=0, has_side_effects=True, vmem_limit_bytes=60 * 1024 * 1024),
        name="layer",
    )(
        inputs, norm_gain.reshape(8, 1, 256), cosine, sine, query_weight, key_weight, value_weight,
        memory_query_weight, memory_key_weight, memory_value_weight, input_gate_weight,
        forget_gate_weight, forget_bias, decay_shift, lambdas,
        jnp.concatenate([head_gain, head_gain]).reshape(1, 128),
        out_weight_attention, out_weight_memory,
    )


def solution(mesh):
    split = P(None, "tp")
    placed = (
        P("sp", "tp"), P(), split, split, split, split, split, split, split, split,
        P("tp"), P("sp", "tp"), P("tp"), P(), P("tp", None), P("tp", None),
    )
    return jax.shard_map(
        per_device, mesh=mesh, in_specs=placed, out_specs=P("sp", "tp"), check_vma=False)
```

time: 315 us -> 107 us (0.34)
  matrix products: 100 us -> 0 us
  Pallas kernels: 0 us -> 98.8 us
  other arithmetic: 55.2 us -> 1.43 us
  waiting for transfers between devices: 53.6 us -> 0 us
  blocking collectives: 45.6 us -> 0 us
  local copies, waits for them, and re-layouts: 28 us -> 6.79 us
  starting transfers between devices: 17.1 us -> 0 us
  between operations: 14 us -> 0.02 us
    dot_general x22 -> x0, matrix products: 100 us -> none  [the longest x2 47.4 us: attend(): jnp.einsum('qhd,khd->hqk', query_side, key_side, preferred_element_type=j...]
    pallas_call x0 -> x1, Pallas kernels: none -> 98.8 us  [per_device(): pl.pallas_call(layer_kernel, out_shape=jax.ShapeDtypeStruct((rows, column...]
    all_to_all x2 -> x0, waiting for transfers between devices: 32 us -> none  [from_everyone(): lax.all_to_all(jnp.broadcast_to(array[None], (devices, *array.shape)), ax...]
    reduce_sum x3 -> x0, other arithmetic: 28.1 us -> none  [the longest x1 26.7 us: attend(): totals = jnp.sum(weights, axis=2)]
    all_to_all x1 -> x0, blocking collectives: 23.5 us -> none  [sum_at_owner(): lax.all_to_all(pieces, axis, split_axis=0, concat_axis=0, tiled=True)]
    all_gather x1 -> x0, blocking collectives: 22.1 us -> none  [gather_axes(): filled = lax.all_gather(filled, axes[number], axis=dim, tiled=True)]
    all_gather x1 -> x0, waiting for transfers between devices: 21.5 us -> none  [gather_axes(): filled = lax.all_gather(filled, axes[number], axis=dim, tiled=True)]
    all_to_all x2 -> x0, starting transfers between devices: 17.1 us -> none  [from_everyone(): lax.all_to_all(jnp.broadcast_to(array[None], (devices, *array.shape)), ax...]
  transfers between devices with their start and end apart: 3 -> 0, of which waited for: 3 -> 0; matrix products, arithmetic and copies ran while one was open for 17% -> 0% of each run, Pallas kernels for 0% -> 0%
where the time goes in v1:
time: 107 us
  Pallas kernels  98.8 us (92%)
  local copies, waits for them, and re-layouts  6.79 us (6%)
  other arithmetic  1.43 us (1%)
    pallas_call x1, Pallas kernels, per_device(): pl.pallas_call(layer_kernel, out_shape=jax.ShapeDtypeStruct((rows, column...  98.8 us
    unnamed x12, local copies, waits for them, and re-layouts  4.59 us

profile of v1, /device:TPU:1, one launch (start us, length us, event | category | flops | bytes accessed | tf_op | source)
XLA Modules:
  0.0 107.1 jit_solution(16889178377252881088)
XLA Ops:
  0.0 0.8 multiply_sine_fusion
  0.8 1.1 %concatenate.10.sine = f32[384,128]{1,0:T(8,128)} concatenate(f32[384,16]{1,0:T(8,128)S(1)} %get-tuple-element.6, f32[384,16]{1,0:T(8,128)S(1)} %get-tuple-element.5, f32[384,16]{1,0:T(8,128)S(1)} %get-tuple-element.6, f32[384,16]{1,0:T(8,128)S(1)} %get-tuple-element.5, f32[384,16]{1,0:T(8,128)S(1)} %get-tuple-element.6, f32[384,16]{1,0:T(8,128)S(1)} %get-tuple-element.5, ...), dimensions={1} | concatenate | bytes 393216 | tf_op jit(solution)/shard_map/concatenate | solution.py:499
  1.9 0.0 copy-start
  1.9 1.1 %concatenate.9.cosine = f32[384,128]{1,0:T(8,128)} concatenate(f32[384,16]{1,0:T(8,128)S(1)} %get-tuple-element.7, f32[384,16]{1,0:T(8,128)S(1)} %get-tuple-element.7, f32[384,16]{1,0:T(8,128)S(1)} %get-tuple-element.7, f32[384,16]{1,0:T(8,128)S(1)} %get-tuple-element.7, f32[384,16]{1,0:T(8,128)S(1)} %get-tuple-element.7, f32[384,16]{1,0:T(8,128)S(1)} %get-tuple-element.7, ...), dimensions={1} | concatenate | bytes 393216 | tf_op jit(solution)/shard_map/concatenate | solution.py:498
  3.0 0.0 copy-done
  3.0 0.0 copy-start.1
  3.0 1.1 copy.21.wig
  4.1 0.0 copy-done.1
  4.1 0.0 copy-start.2
  4.1 1.1 copy.22.wfg
  5.1 0.0 copy-done.2
  5.1 0.0 copy-start.3
  5.1 0.8 copy.23.decay
  6.0 0.0 copy-done.3
  6.0 0.7 maximum_bitcast_fusion.head_gain
  6.6 98.8 %layer.1 = bf16[384,256]{1,0:T(8,128)(2,1)} custom-call(bf16[384,256]{1,0:T(8,128)(2,1)} %x.1, f32[8,1,256]{2,1,0:T(1,128)} %bitcast.3, f32[384,128]{1,0:T(8,128)} %concatenate.9.cosine, f32[384,128]{1,0:T(8,128)} %concatenate.10.sine, bf16[2048,128]{1,0:T(8,128)(2,1)} %wq.1, bf16[2048,128]{1,0:T(8,128)(2,1)} %wk.1, bf16[2048,128]{1,0:T(8,128)(2,1)} %wv.1, ...), custom_call_target="tpu_custom_call" | custom-call | tf_op jit(solution)/shard_map/layer/pallas_call | solution.py:542
  105.5 1.6 %copy.25 = bf16[384,256]{1,0:T(8,128)(2,1)} copy(bf16[384,256]{1,0:T(8,128)(2,1)} %layer.1) | data formatting | bytes 393216
  (2 shorter events, 0.0 us)
Async XLA Ops:
  1.9 1.1 %copy-start = (bf16[2048,2]{0,1:T(2,128)(2,1)S(1)}, bf16[2048,2]{0,1:T(2,128)(2,1)}, u32[]{:S(2)}) copy-start(bf16[2048,2]{0,1:T(2,128)(2,1)} %param.24) | copy-start | bytes 24580
  3.0 1.1 copy-start.1
  4.1 1.1 copy-start.2
  5.1 0.8 copy-start.3

commit v2 on v1

--- a/solution.py
+++ b/solution.py
@@ -1,4 +1,5 @@
 import jax
+import numpy as np
 import jax.numpy as jnp
 from jax import lax
 from jax.experimental import pallas as pl
@@ -13,25 +14,11 @@
 LOG2E = 1.4426950408889634
 SPANS = 32
 ROUNDS = 5
-CHUNKS = 4
+X_LAG = 2
+RELAY_LAG = 1
 MESH = pl.DeviceIdType.MESH
 F32 = jnp.float32
 BF16 = jnp.bfloat16
-
-
-def ring_position(ring, span):
-    a, b = span // 4, span % 4
-    if ring == 0:
-        return 4 * a + (a + b) % 4
-    r = (a + 5 * b) % 8
-    return 4 * (b + 4 * (r // 4)) + r % 4
-
-
-def span_on_ring(ring, position):
-    u, r = position // 4, position % 4
-    if ring == 0:
-        return 4 * u + (r + 32 - u) % 4
-    return 4 * ((3 * u + r) % 8) + u % 4
 
 
 def dot(a, b):
@@ -55,16 +42,15 @@
 
 
 def layer_kernel(
-    x, gain, cosine, sine, wq, wk, wv, wmq, wmk, wmv, wig, wfg, bias, decay, lambdas, head_gain,
+    x, gain, near_table, far_table, wq, wk, wv, wmq, wmk, wmv, wig, wfg, bias, decay, lambdas, head_gain,
     woa, wom, out,
-    xg, xs, squares, w, wi, wf, wo, held, qs, mq, mk, mv, gates, acc, top, st_in, st_out, st_before,
+    xg, xs, squares, w, wo, held, qs, mq, mk, mv, gates, gate_rows, acc, top, st_in, st_out, st_before,
     num_local, log_local, cat, to_partner, from_partner, to_ring, from_ring,
-    load_sem, gather_send, gather_recv, ring_send, ring_recv, scan_send, scan_recv,
+    load_sem, gather_send, gather_recv, z_send, z_recv, x_send, x_recv, scan_send, scan_recv,
     pair_send, pair_recv, sum_send, sum_recv,
 ):
     rows = x.shape[0]
     half_rows = rows // 2
-    chunk = rows // CHUNKS
     sp = lax.axis_index("sp")
     tp = lax.axis_index("tp")
     y, c = tp // 2, tp % 2
@@ -72,9 +58,12 @@
     left = 2 * ((y + 3) % 4) + c
     across = 2 * ((y + 2) % 4) + c
     partner = 2 * y + 1 - c
-    t0, t1 = ring_position(0, sp), ring_position(1, sp)
-    nexts = [span_on_ring(ring, (t + step) % SPANS)
-             for ring, t in ((0, t0), (1, t1)) for step in (1, SPANS - 1)]
+    z, across_x = sp // 4, sp % 4
+    above, below = 4 * ((z + 1) % 8) + across_x, 4 * ((z + 7) % 8) + across_x
+    nexts = [above, below, 4 * z + (across_x + 1) % 4, 4 * z + (across_x + 3) % 4]
+
+    def span_at(dz, dx):
+        return 4 * ((z + dz + 16) % 8) + (across_x + dx) % 4
 
     def remote(src, dst, send, recv, span, seat):
         return pltpu.make_async_remote_copy(
@@ -88,8 +77,6 @@
             ((wq, 0, 0), (wk, 0, 128), (wv, 1, 0), (wmq, 1, 128), (wmk, 2, 0), (wmv, 2, 128))):
         loads.append(pltpu.make_async_copy(
             weight, w.at[tile, :, pl.ds(at, 128)], load_sem.at[1 + number]))
-    loads.append(pltpu.make_async_copy(wig, wi, load_sem.at[7]))
-    loads.append(pltpu.make_async_copy(wfg, wf, load_sem.at[8]))
     for load in loads:
         load.start()
     out_loads = []
@@ -181,10 +168,15 @@
     low = lane < HEAD
     former = lane % 32 < 16
 
+    far_cosine, far_sine = far_table[sp, 0:1, :], far_table[sp, 1:2, :]
+    cosine = far_cosine * near_table[0] - far_sine * near_table[1]
+    sine = far_sine * near_table[0] + far_cosine * near_table[1]
+    sine = jnp.where(former, -sine, sine)
+
     def rotated(flat):
         floats = flat.astype(BF16).astype(F32)
         swapped = jnp.where(former, pltpu.roll(floats, 112, 1), pltpu.roll(floats, 16, 1))
-        return (floats * cosine[...] + swapped * sine[...]).astype(BF16).astype(F32)
+        return (floats * cosine + swapped * sine).astype(BF16).astype(F32)
 
     product = dot(scaled, w[0]) * inverse
     queries = rotated(product[:, :128])
@@ -192,31 +184,42 @@
     product = dot(scaled, w[1]) * inverse
     values = product[:, :128].astype(BF16).astype(F32)
     mq[...] = product[:, 128:].astype(BF16)
-    held[0, t0] = jnp.where(low, keys, pltpu.roll(values, 64, 1)).astype(BF16)
-    held[1, t1] = jnp.where(low, pltpu.roll(keys, 64, 1), values).astype(BF16)
+    held[0, sp] = jnp.where(low, keys, pltpu.roll(values, 64, 1)).astype(BF16)
+    held[1, sp] = jnp.where(low, pltpu.roll(keys, 64, 1), values).astype(BF16)
     for head in range(2):
         turned = queries if head == 0 else pltpu.roll(queries, 64, 1)
         for side in range(2):
             inside = (lane >= DD * side) & (lane < DD * side + DD)
             qs[head, side * rows:(side + 1) * rows, :] = jnp.where(inside, turned, 0.0).astype(BF16)
 
-    def passing(stream, step, number):
-        ring, way = stream // 2, stream % 2
-        t = (t0, t1)[ring]
-        origin = (t + SPANS - step) % SPANS if way == 0 else (t + step) % SPANS
-        ref = held.at[ring, origin, pl.ds(number * chunk, chunk), :]
-        return remote(ref, ref, ring_send.at[stream, number],
-                      ring_recv.at[stream, step, number], nexts[stream], tp)
-
-    for number in range(CHUNKS):
-        for stream in range(4):
-            passing(stream, 0, number).start()
+    def z_copy(chain, way, hop, dx):
+        dz = 1 - hop if way == 0 else hop - 1
+        ref = held.at[1 if isinstance(chain, int) and chain == 0 else 0, span_at(dz, dx)]
+        return remote(ref, ref, z_send.at[chain, way, hop - 1], z_recv.at[chain, way, hop - 1],
+                      nexts[way], tp)
+
+    def x_copy(number, kind, ring, dz):
+        if kind < 2:
+            ref = held.at[ring, span_at(dz, 0)]
+        else:
+            ref = held.at[ring, span_at(dz, 3 if kind == 2 else 1),
+                          pl.ds((kind - 2) * half_rows, half_rows), :]
+        return remote(ref, ref, x_send.at[number, kind], x_recv.at[number, kind],
+                      nexts[2 + kind % 2], tp)
+
+    for way in range(2):
+        z_copy(0, way, 1, 0).start()
+        x_copy(5, way, 0, 0).start()
+    for way in range(2):
+        z_copy(1, way, 1, 0).start()
+        x_copy(0, way, 1, 0).start()
 
     product = dot(scaled, w[2]) * inverse
     mk[...] = product[:, :128].astype(BF16)
     mv[...] = product[:, 128:].astype(BF16)
-    gate_in = dot(scaled, wi[...]) * inverse
-    forget = dot(scaled, wf[...]) * inverse
+    inverse_row = jnp.transpose(jnp.broadcast_to(inverse, (rows, 128)))[0:1, :]
+    gate_in = dot_t(wig[...], scaled) * inverse_row
+    forget = dot_t(wfg[...], scaled) * inverse_row
 
     def log_sigmoid(a):
         return jnp.minimum(a, 0.0) - jnp.log1p(jnp.exp(-jnp.abs(a)))
@@ -224,17 +227,22 @@
     def per_head(parts):
         return jnp.where(low, parts[0], parts[1])
 
-    log_forget = per_head([
-        log_sigmoid(forget[:, h:h + 1] + bias[h]) + decay[:, h:h + 1] for h in range(2)])
-    gate = per_head([gate_in[:, h:h + 1] for h in range(2)])
+    first_row = lax.broadcasted_iota(jnp.int32, (2, rows), 0) == 0
+    log_forget = log_sigmoid(forget + jnp.where(first_row, bias[0], bias[1])) + decay[...]
     before_or_at = (lax.broadcasted_iota(jnp.int32, (rows, rows), 1)
                     <= lax.broadcasted_iota(jnp.int32, (rows, rows), 0))
     triangle = jnp.where(before_or_at, 1.0, 0.0).astype(BF16)
     high, middle, small = thirds(log_forget)
-    cumulative = dot(triangle, high) + dot(triangle, middle) + dot(triangle, small)
-    gates[0] = cumulative
-    gates[1] = gate - cumulative
-    span_decay = cumulative[rows - 1:rows, :]
+    cumulative = dot_t(high, triangle) + dot_t(middle, triangle) + dot_t(small, triangle)
+    gate_rows[...] = gate_in - cumulative
+    upper_rows = lax.broadcasted_iota(jnp.int32, (128, rows), 0) < HEAD
+
+    def columns(pair):
+        return jnp.transpose(jnp.where(upper_rows, pair[0:1, :], pair[1:2, :]))
+
+    gates[0] = columns(cumulative)
+    gates[1] = columns(gate_rows[...])
+    span_decay = gates[0, rows - 1:rows, :]
     toward_end = span_decay + gates[1]
     span_top = jnp.max(toward_end, axis=0, keepdims=True)
     end_weights = jnp.exp(toward_end - span_top)
@@ -292,16 +300,23 @@
         top[ring] = highest
 
     causal = jnp.concatenate([before_or_at, before_or_at], axis=0)
-    visit(0, t0, causal)
+    visit(0, sp, causal)
     scan_copy(0).start()
-    visit(1, t1, causal)
+    x_copy(5, 0, 0, 0).wait_recv()
+    x_copy(5, 2, 0, 0).start()
+    for way in range(2):
+        z_copy(2, way, 1, 3).start()
+    x_copy(5, 1, 0, 0).wait_recv()
+    x_copy(5, 3, 0, 0).start()
+    for way in range(2):
+        z_copy(3, way, 1, 1).start()
+    visit(1, sp, causal)
 
     def local_memory():
         sums, tops, totals = [], [], []
-        turned = jnp.transpose(gates[1])
         for head in range(2):
             inside = low if head == 0 else ~low
-            gap = gates[0][:, HEAD * head:HEAD * head + 1] + turned[HEAD * head:HEAD * head + 1, :]
+            gap = gates[0, :, HEAD * head:HEAD * head + 1] + gate_rows[head:head + 1, :]
             gap = jnp.where(before_or_at, gap, NEGATIVE)
             highest = jnp.max(gap, axis=1, keepdims=True)
             within = jnp.exp(gap - highest)
@@ -334,65 +349,131 @@
             st_out[number + 1, 0:HEAD, :] = jnp.where(reached, whole[0], mine[0])
             st_out[number + 1, HEAD:HEAD + 8, :] = jnp.where(reached, whole[1], mine[1])
 
-    def step_body(step, unused):
-        def sub_step(number, unused):
-            for stream in range(4):
-                if stream % 2 == 0:
-                    passing(stream, step - 1, number).wait_recv()
-
-                    @pl.when(step < 16)
-                    def _():
-                        passing(stream, step - 1, number).wait_send()
-                        passing(stream, step, number).start()
-                else:
-                    @pl.when(step < 16)
-                    def _():
-                        passing(stream, step - 1, number).wait_recv()
-
-                    @pl.when(step < 15)
-                    def _():
-                        passing(stream, step - 1, number).wait_send()
-                        passing(stream, step, number).start()
-            if CHUNKS == 4:
-                attend_stream(step - 1, number)
-            else:
-                for k in range(4 // CHUNKS):
-                    attend_stream(step - 1, number * (4 // CHUNKS) + k)
+    def attend(ring, dz, dx, valid):
+        origin = span_at(dz, dx)
+
+        @pl.when(valid & (origin < sp))
+        def _():
+            visit(ring, origin)
+
+    def iteration(i, unused):
+        pair, hop = i % 2, i // 2 + 1
+
+        def by_way(ups, downs, then):
+            def body(way, unused):
+                pl.when(way == 0)(ups)
+                pl.when(way == 1)(downs)
+                then(way)
+                return unused
+
+            lax.fori_loop(0, 2, body, 0)
+
+        def signed(way, distance):
+            return (2 * way - 1) * distance
+
+        @pl.when((i >= 1) & (i < ROUNDS))
+        def _():
+            scan_copy(i).start()
+
+        def own_chain(way):
+            last = 4 - way
+
+            @pl.when(i < last)
+            def _():
+                z_copy(0, way, i + 1, 0).wait_recv()
+
+                @pl.when(i < last - 1)
+                def _():
+                    z_copy(0, way, i + 2, 0).start()
+
+                for kind in range(2):
+                    x_copy(5 * way + i + 1, kind, 1, (2 * way - 1) * (i + 1)).start()
+
+        by_way(lambda: own_chain(0), lambda: own_chain(1),
+               lambda way: attend(1, signed(way, i + 1), 0, i < 4 - way))
+
+        def x_arrival(rows_way, kind):
+            valid = (i <= 4) if rows_way == 0 else (i >= 1) & (i <= 3)
+
+            @pl.when(valid)
+            def _():
+                dz = (2 * rows_way - 1) * i
+                x_copy(5 * rows_way + i, kind, 1, dz).wait_recv()
+                x_copy(5 * rows_way + i, kind + 2, 1, dz).start()
+
+        def x_attend(rows_way, side):
+            j = i - X_LAG
+            valid = (j >= 0) & (j <= 4) if rows_way == 0 else (j >= 1) & (j <= 3)
+            attend(1, (2 * rows_way - 1) * j, 3 - 2 * side, valid)
+
+        by_way(lambda: x_arrival(0, 0), lambda: x_arrival(0, 1), lambda side: x_attend(0, side))
+
+        @pl.when(i == 0)
+        def _():
+            x_copy(5, 2, 0, 0).wait_recv()
+            x_copy(5, 3, 0, 0).wait_recv()
+            for way in range(2):
+                z_copy(4, way, 1, 2).start()
+
+        def chain(number, way, dx, last):
+            @pl.when(hop <= last)
+            def _():
+                z_copy(number, way, hop, dx).wait_recv()
+
+                @pl.when(hop < last)
+                def _():
+                    z_copy(number, way, hop + 1, dx).start()
+
+        first = 1 + 2 * pair
+        by_way(lambda: chain(first, 0, pair, 4), lambda: chain(first, 1, pair, 3),
+               lambda way: attend(0, signed(way, hop), pair, hop <= 4 - way))
+        by_way(lambda: x_arrival(1, 0), lambda: x_arrival(1, 1), lambda side: x_attend(1, side))
+        by_way(lambda: chain(first + 1, 0, 3 - pair, 3), lambda: chain(first + 1, 1, 3 - pair, 4),
+               lambda way: attend(0, signed(way, hop), 3 - pair, hop <= 3 + way))
+
+        def relayed(rows_way):
+            j = i - 1
+            valid = (j >= 0) & (j <= 4) if rows_way == 0 else (j >= 1) & (j <= 3)
+
+            @pl.when(valid)
+            def _():
+                for kind in (2, 3):
+                    x_copy(5 * rows_way + j, kind, 1, (2 * rows_way - 1) * j).wait_recv()
+
+        def relay_attend(way):
+            j = i - 1 - RELAY_LAG
+            own = way == 2
+            valid = jnp.where(own, i < 3, (j >= way) & (j <= 4 - way))
+            attend(jnp.where(own, 0, 1), jnp.where(own, 0, signed(way, j)),
+                   jnp.where(own, 3 - i, 2), valid)
+
+        def body(way, unused):
+            pl.when(way == 0)(lambda: relayed(0))
+            pl.when(way == 1)(lambda: relayed(1))
+            relay_attend(way)
             return unused
 
-        lax.fori_loop(0, CHUNKS, sub_step, 0)
-
-        @pl.when(step == 1)
+        lax.fori_loop(0, 3, body, 0)
+
+        @pl.when(i == 0)
         def _():
             local_memory()
 
-        @pl.when((step % 3 == 2) & (step < 15))
+        @pl.when(i < ROUNDS)
         def _():
-            scan_round(step // 3)
-
-        @pl.when((step % 3 == 0) & (step < 13))
-        def _():
-            scan_copy(step // 3).start()
+            scan_round(i)
 
         return unused
 
-    def attend_stream(step, stream):
-        ring, way = stream // 2, stream % 2
-        start = t0 + ring * (t1 - t0)
-        position = (start + way * (2 * step) + SPANS - step) % SPANS
-        first, second = span_on_ring(0, position), span_on_ring(1, position)
-        origin = first + ring * (second - first)
-
-        @pl.when(origin < sp)
-        def _():
-            visit(ring, position)
-
-    lax.fori_loop(1, 17, step_body, 0)
-    for number in range(CHUNKS):
-        for stream in range(4):
-            passing(stream, 15 if stream % 2 == 0 else 14, number).wait_send()
-    attend_stream(16, 0)
-    attend_stream(16, 2)
+    lax.fori_loop(0, 8, iteration, 0)
+    for number in range(5):
+        for way in range(2):
+            last = 4 if (number in (2, 4)) == (way == 1) else 3
+            for hop in range(1, last + 1):
+                z_copy(number, way, hop, 0).wait_send()
+    for number in (0, 1, 2, 3, 4, 5, 6, 7, 8):
+        for kind in range(4):
+            x_copy(number, kind, 1, 0).wait_send()
     for number in range(ROUNDS):
         scan_copy(number).wait_send()
 
@@ -407,7 +488,7 @@
         mean = jnp.sum(squared, axis=1, keepdims=True) * (1.0 / HEAD)
         rooted.append(difference * lax.rsqrt(mean + EPSILON))
     cat[:, 0:128] = (jnp.where(low, pltpu.roll(rooted[0], 64, 1), rooted[1])
-                     * head_gain[...]).astype(BF16)
+                     * jnp.concatenate([head_gain[...]] * 2, axis=1)).astype(BF16)
 
     start_memory = jnp.zeros((HEAD, 128), F32)
     start_tail = jnp.zeros((8, 128), F32)
@@ -490,13 +571,12 @@
     decay_shift, lambdas, head_gain, out_weight_attention, out_weight_memory,
 ):
     rows, columns = inputs.shape
-    positions = (lax.axis_index("sp") * rows + jnp.arange(rows, dtype=jnp.int32)).astype(F32)
     middle = DD // 2
-    inverse = 1.0 / ROTARY_BASE ** (jnp.arange(middle, dtype=F32) / middle)
-    angles = positions[:, None] * inverse[None, :]
-    cosine, sine = jnp.cos(angles), jnp.sin(angles)
-    cosine = jnp.concatenate([cosine] * 8, axis=1)
-    sine = jnp.concatenate([-sine, sine] * 4, axis=1)
+    inverse = 1.0 / ROTARY_BASE ** (np.arange(middle) / middle)
+    near = np.tile(np.arange(rows)[:, None] * inverse[None, :], (1, 8))
+    far = np.tile((np.arange(SPANS) * rows)[:, None] * inverse[None, :], (1, 8))
+    near = jnp.asarray(np.stack([np.cos(near), np.sin(near)]), F32)
+    far = jnp.asarray(np.stack([np.cos(far), np.sin(far)], axis=1), F32)
     vmem = pl.BlockSpec(memory_space=pltpu.VMEM)
     smem = pl.BlockSpec(memory_space=pltpu.SMEM)
     anywhere = pl.BlockSpec(memory_space=pl.ANY)
@@ -506,8 +586,6 @@
         pltpu.VMEM((8, rows, columns), BF16),
         pltpu.VMEM((rows, columns), F32),
         pltpu.VMEM((3, 2048, 256), BF16),
-        pltpu.VMEM((2048, 2), BF16),
-        pltpu.VMEM((2048, 2), BF16),
         pltpu.VMEM((8, 256, 256), BF16),
         pltpu.VMEM((2, SPANS, rows, 128), BF16),
         pltpu.VMEM((2, 2 * rows, 128), BF16),
@@ -515,6 +593,7 @@
         pltpu.VMEM((rows, 128), BF16),
         pltpu.VMEM((rows, 128), BF16),
         pltpu.VMEM((2, rows, 128), F32),
+        pltpu.VMEM((2, rows), F32),
         pltpu.VMEM((2, 2 * rows, 128), F32),
         pltpu.VMEM((2, 2 * rows, 128), F32),
         pltpu.VMEM((ROUNDS, HEAD + 8, 128), F32),
@@ -530,8 +609,10 @@
         pltpu.SemaphoreType.DMA((25,)),
         pltpu.SemaphoreType.DMA((13,)),
         pltpu.SemaphoreType.DMA((13,)),
-        pltpu.SemaphoreType.DMA((4, CHUNKS)),
-        pltpu.SemaphoreType.DMA((4, 16, CHUNKS)),
+        pltpu.SemaphoreType.DMA((5, 2, 4)),
+        pltpu.SemaphoreType.DMA((5, 2, 4)),
+        pltpu.SemaphoreType.DMA((10, 4)),
+        pltpu.SemaphoreType.DMA((10, 4)),
         pltpu.SemaphoreType.DMA((ROUNDS,)),
         pltpu.SemaphoreType.DMA((ROUNDS,)),
         pltpu.SemaphoreType.DMA((4,)),
@@ -542,7 +623,7 @@
     return pl.pallas_call(
         layer_kernel,
         out_shape=jax.ShapeDtypeStruct((rows, columns), BF16),
-        in_specs=[anywhere, vmem, vmem, vmem] + [anywhere] * 8
+        in_specs=[anywhere, vmem, vmem, vmem] + [anywhere] * 6 + [vmem, vmem]
         + [smem, vmem, smem, vmem, anywhere, anywhere],
         out_specs=vmem,
         scratch_shapes=scratch,
@@ -550,10 +631,9 @@
             collective_id=0, has_side_effects=True, vmem_limit_bytes=60 * 1024 * 1024),
         name="layer",
     )(
-        inputs, norm_gain.reshape(8, 1, 256), cosine, sine, query_weight, key_weight, value_weight,
-        memory_query_weight, memory_key_weight, memory_value_weight, input_gate_weight,
-        forget_gate_weight, forget_bias, decay_shift, lambdas,
-        jnp.concatenate([head_gain, head_gain]).reshape(1, 128),
+        inputs, norm_gain.reshape(8, 1, 256), near, far, query_weight, key_weight, value_weight,
+        memory_query_weight, memory_key_weight, memory_value_weight, input_gate_weight.T,
+        forget_gate_weight.T, forget_bias, decay_shift.T, lambdas, head_gain.reshape(1, HEAD),
         out_weight_attention, out_weight_memory,
     )
 

time: 107 us -> 89.1 us (0.83)
  the two profiles are of different devices: /device:TPU:1 before, /device:TPU:193 now
where the time goes in v2:
time: 89.1 us; the launch traced here: 88.9 us
  Pallas kernels  87.3 us (98%)
  local copies, waits for them, and re-layouts  1.62 us (2%)
    pallas_call x1, Pallas kernels, per_device(): pl.pallas_call(layer_kernel, out_shape=jax.ShapeDtypeStruct((rows, column...  87.3 us

profile of v2, /device:TPU:193, one launch (start us, length us, event | category | flops | bytes accessed | tf_op | source)
XLA Modules:
  0.0 88.9 jit_solution(6811635396873605137)
XLA Ops:
  0.0 87.3 %layer.1 = bf16[384,256]{1,0:T(8,128)(2,1)} custom-call(bf16[384,256]{1,0:T(8,128)(2,1)} %x.1, f32[8,1,256]{2,1,0:T(1,128)} %bitcast.5, f32[2,384,128]{2,1,0:T(8,128)} %constant.4.clone.near_table, f32[32,2,128]{2,1,0:T(2,128)} %constant.5.clone.far_table, bf16[2048,128]{1,0:T(8,128)(2,1)} %wq.1, bf16[2048,128]{1,0:T(8,128)(2,1)} %wk.1, ...), custom_call_target="tpu_custom_call" | custom-call | tf_op jit(solution)/shard_map/layer/pallas_call | solution.py:623
  87.3 1.6 %copy.20 = bf16[384,256]{1,0:T(8,128)(2,1)} copy(bf16[384,256]{1,0:T(8,128)(2,1)} %layer.1) | data formatting | bytes 393216

commit v3 on v2

--- a/solution.py
+++ b/solution.py
@@ -42,11 +42,12 @@
 
 
 def layer_kernel(
-    x, gain, near_table, far_table, wq, wk, wv, wmq, wmk, wmv, wig, wfg, bias, decay, lambdas, head_gain,
-    woa, wom, out,
+    x, gain_in, near_in, far_in, wq, wk, wv, wmq, wmk, wmv, wig_in, wfg_in, bias_in, decay_in,
+    lambdas_in, head_gain_in, woa, wom, out,
+    gain, near_table, far_table, wig, wfg, bias, decay, lambdas, head_gain,
     xg, xs, squares, w, wo, held, qs, mq, mk, mv, gates, gate_rows, acc, top, st_in, st_out, st_before,
     num_local, log_local, cat, to_partner, from_partner, to_ring, from_ring,
-    load_sem, gather_send, gather_recv, z_send, z_recv, x_send, x_recv, scan_send, scan_recv,
+    small_sem, load_sem, gather_send, gather_recv, z_send, z_recv, x_send, x_recv, scan_send, scan_recv,
     pair_send, pair_recv, sum_send, sum_recv,
 ):
     rows = x.shape[0]
@@ -70,6 +71,15 @@
             src_ref=src, dst_ref=dst, send_sem=send, recv_sem=recv,
             device_id=(span, seat), device_id_type=MESH)
 
+    barrier = pltpu.get_barrier_semaphore()
+    greeted = [(sp, right), (sp, left), (sp, partner)] + [(span, tp) for span in nexts]
+    for number in range(ROUNDS):
+        greeted.append(((sp + 2 ** number) % SPANS, tp))
+        if number < ROUNDS - 1:
+            greeted.append(((sp + SPANS - 2 ** number) % SPANS, tp))
+    for span, seat in greeted:
+        pl.semaphore_signal(barrier, inc=1, device_id=(span, seat), device_id_type=MESH)
+
     own_load = pltpu.make_async_copy(x, xg.at[tp], load_sem.at[0])
     own_load.start()
     loads = []
@@ -77,6 +87,13 @@
             ((wq, 0, 0), (wk, 0, 128), (wv, 1, 0), (wmq, 1, 128), (wmk, 2, 0), (wmv, 2, 128))):
         loads.append(pltpu.make_async_copy(
             weight, w.at[tile, :, pl.ds(at, 128)], load_sem.at[1 + number]))
+    small_loads = {}
+    for number, (source, target) in enumerate((
+            (gain_in, gain), (near_in, near_table), (far_in.at[sp], far_table), (wig_in, wig),
+            (wfg_in, wfg), (bias_in, bias), (decay_in, decay), (lambdas_in, lambdas),
+            (head_gain_in, head_gain))):
+        small_loads[number] = pltpu.make_async_copy(source, target, small_sem.at[number])
+        small_loads[number].start()
     for load in loads:
         load.start()
     out_loads = []
@@ -88,14 +105,6 @@
     for load in out_loads:
         load.start()
 
-    barrier = pltpu.get_barrier_semaphore()
-    greeted = [(sp, right), (sp, left), (sp, partner)] + [(span, tp) for span in nexts]
-    for number in range(ROUNDS):
-        greeted.append(((sp + 2 ** number) % SPANS, tp))
-        if number < ROUNDS - 1:
-            greeted.append(((sp + SPANS - 2 ** number) % SPANS, tp))
-    for span, seat in greeted:
-        pl.semaphore_signal(barrier, inc=1, device_id=(span, seat), device_id_type=MESH)
     pl.semaphore_wait(barrier, len(greeted))
 
     def piece(seat, half):
@@ -129,6 +138,7 @@
         xs[seat] = (block * gain[seat]).astype(BF16)
 
     squares[...] = jnp.zeros_like(squares)
+    small_loads[0].wait()
     absorb(tp)
     sends[0].wait_recv()
     sends[5].start()
@@ -158,7 +168,7 @@
     absorb(2 * ((y + 2) % 4) + 1 - c)
     for number in range(13):
         sends[number].wait_send()
-    for load in loads:
+    for load in loads + [small_loads[number] for number in range(1, 9)]:
         load.wait()
 
     inverse = lax.rsqrt(
@@ -168,7 +178,7 @@
     low = lane < HEAD
     former = lane % 32 < 16
 
-    far_cosine, far_sine = far_table[sp, 0:1, :], far_table[sp, 1:2, :]
+    far_cosine, far_sine = far_table[0:1, :], far_table[1:2, :]
     cosine = far_cosine * near_table[0] - far_sine * near_table[1]
     sine = far_sine * near_table[0] + far_cosine * near_table[1]
     sine = jnp.where(former, -sine, sine)
@@ -186,12 +196,6 @@
     mq[...] = product[:, 128:].astype(BF16)
     held[0, sp] = jnp.where(low, keys, pltpu.roll(values, 64, 1)).astype(BF16)
     held[1, sp] = jnp.where(low, pltpu.roll(keys, 64, 1), values).astype(BF16)
-    for head in range(2):
-        turned = queries if head == 0 else pltpu.roll(queries, 64, 1)
-        for side in range(2):
-            inside = (lane >= DD * side) & (lane < DD * side + DD)
-            qs[head, side * rows:(side + 1) * rows, :] = jnp.where(inside, turned, 0.0).astype(BF16)
-
     def z_copy(chain, way, hop, dx):
         dz = 1 - hop if way == 0 else hop - 1
         ref = held.at[1 if isinstance(chain, int) and chain == 0 else 0, span_at(dz, dx)]
@@ -214,6 +218,11 @@
         z_copy(1, way, 1, 0).start()
         x_copy(0, way, 1, 0).start()
 
+    for head in range(2):
+        turned = queries if head == 0 else pltpu.roll(queries, 64, 1)
+        for side in range(2):
+            inside = (lane >= DD * side) & (lane < DD * side + DD)
+            qs[head, side * rows:(side + 1) * rows, :] = jnp.where(inside, turned, 0.0).astype(BF16)
     product = dot(scaled, w[2]) * inverse
     mk[...] = product[:, :128].astype(BF16)
     mv[...] = product[:, 128:].astype(BF16)
@@ -412,8 +421,7 @@
         def _():
             x_copy(5, 2, 0, 0).wait_recv()
             x_copy(5, 3, 0, 0).wait_recv()
-            for way in range(2):
-                z_copy(4, way, 1, 2).start()
+            z_copy(4, 0, 1, 2).start()
 
         def chain(number, way, dx, last):
             @pl.when(hop <= last)
@@ -425,11 +433,31 @@
                     z_copy(number, way, hop + 1, dx).start()
 
         first = 1 + 2 * pair
-        by_way(lambda: chain(first, 0, pair, 4), lambda: chain(first, 1, pair, 3),
-               lambda way: attend(0, signed(way, hop), pair, hop <= 4 - way))
+
+        def first_downwards():
+            chain(first, 1, pair, 4)
+
+            @pl.when(pair == 1)
+            def _():
+                x_copy(9 + hop, 3, 0, hop).start()
+
+        def second_downwards():
+            @pl.when(pair == 0)
+            def _():
+                chain(2, 1, 3, 4)
+                x_copy(9 + hop, 2, 0, hop).start()
+
+            @pl.when((pair == 1) & (hop >= 2))
+            def _():
+                for kind in (2, 3):
+                    x_copy(8 + hop, kind, 0, hop - 1).wait_recv()
+
+        by_way(lambda: chain(first, 0, pair, 3), first_downwards,
+               lambda way: attend(0, signed(way, hop), pair, hop <= 3 + way))
         by_way(lambda: x_arrival(1, 0), lambda: x_arrival(1, 1), lambda side: x_attend(1, side))
-        by_way(lambda: chain(first + 1, 0, 3 - pair, 3), lambda: chain(first + 1, 1, 3 - pair, 4),
-               lambda way: attend(0, signed(way, hop), 3 - pair, hop <= 3 + way))
+        by_way(lambda: chain(first + 1, 0, 3 - pair, 3), second_downwards,
+               lambda way: attend(0, signed(way, hop - pair * way), 3 - pair,
+                                  (hop >= 1 + pair * way) & (hop <= 3 + way)))
 
         def relayed(rows_way):
             j = i - 1
@@ -466,14 +494,19 @@
         return unused
 
     lax.fori_loop(0, 8, iteration, 0)
-    for number in range(5):
-        for way in range(2):
-            last = 4 if (number in (2, 4)) == (way == 1) else 3
+    for kind in (2, 3):
+        x_copy(13, kind, 0, 4).wait_recv()
+    attend(0, 4, 2, sp >= 0)
+    for number, lasts in enumerate(((4, 3), (3, 4), (3, 4), (3, 4), (3, 0))):
+        for way, last in enumerate(lasts):
             for hop in range(1, last + 1):
                 z_copy(number, way, hop, 0).wait_send()
-    for number in (0, 1, 2, 3, 4, 5, 6, 7, 8):
+    for number in range(9):
         for kind in range(4):
             x_copy(number, kind, 1, 0).wait_send()
+    for number in range(10, 14):
+        for kind in (2, 3):
+            x_copy(number, kind, 0, 0).wait_send()
     for number in range(ROUNDS):
         scan_copy(number).wait_send()
 
@@ -528,39 +561,58 @@
         pairs[number].wait_recv()
         return own + from_partner[number].astype(F32)
 
-    def shift(number, seat):
-        return remote(to_ring.at[number], from_ring.at[number], sum_send.at[number],
-                      sum_recv.at[number], sp, seat)
-
-    shifts = [shift(0, right), shift(1, left), shift(2, right), shift(3, right), shift(4, left),
-              shift(5, left)]
+    quarter = half_rows // 2
+
+    def shift(number, seat, part=None):
+        if part is None:
+            source, target = to_ring.at[number], from_ring.at[number]
+        else:
+            span = pl.ds(part * quarter, quarter)
+            source, target = to_ring.at[number, span, :], from_ring.at[number, span, :]
+        lane_of = part or 0
+        return remote(source, target, sum_send.at[number, lane_of], sum_recv.at[number, lane_of],
+                      sp, seat)
+
+    across_right = [shift(0, right, part) for part in range(2)]
+    across_left = [shift(1, left, part) for part in range(2)]
+    along_right, along_left = shift(2, right), shift(4, left)
+    added_right = [shift(3, right, part) for part in range(2)]
+    added_left = [shift(5, left, part) for part in range(2)]
     total = summed(0)
     to_ring[0] = total[:half_rows].astype(BF16)
     to_ring[1] = total[half_rows:].astype(BF16)
-    shifts[0].start()
-    shifts[1].start()
+    for part in range(2):
+        across_right[part].start()
+        across_left[part].start()
     total = summed(1)
     to_ring[2] = total[half_rows:].astype(BF16)
-    shifts[2].start()
+    along_right.start()
     rest = total[:half_rows]
     total = summed(2)
     to_ring[4] = total[:half_rows].astype(BF16)
-    shifts[4].start()
-    shifts[0].wait_recv()
-    to_ring[3] = (rest + from_ring[0].astype(F32)).astype(BF16)
-    shifts[3].start()
-    shifts[1].wait_recv()
-    to_ring[5] = (total[half_rows:] + from_ring[1].astype(F32)).astype(BF16)
-    shifts[5].start()
+    along_left.start()
+    other = total[half_rows:]
     total = summed(3)
-    for number in (2, 4):
-        shifts[number].wait_recv()
+    for part in range(2):
+        span = slice(part * quarter, (part + 1) * quarter)
+        across_right[part].wait_recv()
+        to_ring[3, span, :] = (rest[span] + from_ring[0, span, :].astype(F32)).astype(BF16)
+        added_right[part].start()
+        across_left[part].wait_recv()
+        to_ring[5, span, :] = (other[span] + from_ring[1, span, :].astype(F32)).astype(BF16)
+        added_left[part].start()
+    along_right.wait_recv()
+    along_left.wait_recv()
     lower = total[half_rows:] + from_ring[2].astype(F32)
     upper = total[:half_rows] + from_ring[4].astype(F32)
-    shifts[3].wait_recv()
-    shifts[5].wait_recv()
-    out[0:half_rows, :] = (upper + from_ring[3].astype(F32)).astype(BF16)
-    out[half_rows:rows, :] = (lower + from_ring[5].astype(F32)).astype(BF16)
+    for part in range(2):
+        span = slice(part * quarter, (part + 1) * quarter)
+        added_right[part].wait_recv()
+        out[span, :] = (upper[span] + from_ring[3, span, :].astype(F32)).astype(BF16)
+        added_left[part].wait_recv()
+        out[half_rows + part * quarter:half_rows + (part + 1) * quarter, :] = (
+            lower[span] + from_ring[5, span, :].astype(F32)).astype(BF16)
+    shifts = across_right + across_left + added_right + added_left + [along_right, along_left]
     for copy in pairs + shifts:
         copy.wait_send()
 
@@ -578,10 +630,18 @@
     near = jnp.asarray(np.stack([np.cos(near), np.sin(near)]), F32)
     far = jnp.asarray(np.stack([np.cos(far), np.sin(far)], axis=1), F32)
     vmem = pl.BlockSpec(memory_space=pltpu.VMEM)
-    smem = pl.BlockSpec(memory_space=pltpu.SMEM)
     anywhere = pl.BlockSpec(memory_space=pl.ANY)
     half = rows // 2
     scratch = [
+        pltpu.VMEM((8, 1, columns), F32),
+        pltpu.VMEM((2, rows, 128), F32),
+        pltpu.VMEM((2, 128), F32),
+        pltpu.VMEM((2, 2048), BF16),
+        pltpu.VMEM((2, 2048), BF16),
+        pltpu.SMEM((2,), F32),
+        pltpu.VMEM((2, rows), F32),
+        pltpu.SMEM((2,), F32),
+        pltpu.VMEM((1, HEAD), F32),
         pltpu.VMEM((8, rows, columns), BF16),
         pltpu.VMEM((8, rows, columns), BF16),
         pltpu.VMEM((rows, columns), F32),
@@ -606,25 +666,25 @@
         pltpu.VMEM((4, rows, 256), BF16),
         pltpu.VMEM((6, half, 256), BF16),
         pltpu.VMEM((6, half, 256), BF16),
+        pltpu.SemaphoreType.DMA((9,)),
         pltpu.SemaphoreType.DMA((25,)),
         pltpu.SemaphoreType.DMA((13,)),
         pltpu.SemaphoreType.DMA((13,)),
         pltpu.SemaphoreType.DMA((5, 2, 4)),
         pltpu.SemaphoreType.DMA((5, 2, 4)),
-        pltpu.SemaphoreType.DMA((10, 4)),
-        pltpu.SemaphoreType.DMA((10, 4)),
+        pltpu.SemaphoreType.DMA((14, 4)),
+        pltpu.SemaphoreType.DMA((14, 4)),
         pltpu.SemaphoreType.DMA((ROUNDS,)),
         pltpu.SemaphoreType.DMA((ROUNDS,)),
         pltpu.SemaphoreType.DMA((4,)),
         pltpu.SemaphoreType.DMA((4,)),
-        pltpu.SemaphoreType.DMA((6,)),
-        pltpu.SemaphoreType.DMA((6,)),
+        pltpu.SemaphoreType.DMA((6, 2)),
+        pltpu.SemaphoreType.DMA((6, 2)),
     ]
     return pl.pallas_call(
         layer_kernel,
         out_shape=jax.ShapeDtypeStruct((rows, columns), BF16),
-        in_specs=[anywhere, vmem, vmem, vmem] + [anywhere] * 6 + [vmem, vmem]
-        + [smem, vmem, smem, vmem, anywhere, anywhere],
+        in_specs=[anywhere] * 18,
         out_specs=vmem,
         scratch_shapes=scratch,
         compiler_params=pltpu.CompilerParams(

time: 89.1 us -> 89.6 us (level)
  the two profiles are of different devices: /device:TPU:193 before, /device:TPU:225 now
where the time goes in v3:
time: 89.6 us; the launch traced here: 89.5 us
  Pallas kernels  87.9 us (98%)
  local copies, waits for them, and re-layouts  1.62 us (2%)
    pallas_call x1, Pallas kernels, per_device(): pl.pallas_call(layer_kernel, out_shape=jax.ShapeDtypeStruct((rows, column...  87.9 us

profile of v3, /device:TPU:225, one launch (start us, length us, event | category | flops | bytes accessed | tf_op | source)
XLA Modules:
  0.0 89.5 jit_solution(1139282149137560184)
XLA Ops:
  0.0 87.9 %layer.1 = bf16[384,256]{1,0:T(8,128)(2,1)} custom-call(bf16[384,256]{1,0:T(8,128)(2,1)} %x.1, f32[8,1,256]{2,1,0:T(1,128)} %bitcast.5, f32[2,384,128]{2,1,0:T(8,128)} %constant.4.clone.near_in, f32[32,2,128]{2,1,0:T(2,128)} %constant.5.clone.far_in, bf16[2048,128]{1,0:T(8,128)(2,1)} %wq.1, bf16[2048,128]{1,0:T(8,128)(2,1)} %wk.1, bf16[2048,128]{1,0:T(8,128)(2,1)} %wv.1, ...), custom_call_target="tpu_custom_call" | custom-call | tf_op jit(solution)/shard_map/layer/pallas_call | solution.py:684
  87.9 1.6 %copy.20 = bf16[384,256]{1,0:T(8,128)(2,1)} copy(bf16[384,256]{1,0:T(8,128)(2,1)} %layer.1) | data formatting | bytes 393216

commit v4 on v3

--- a/solution.py
+++ b/solution.py
@@ -73,10 +73,6 @@
 
     barrier = pltpu.get_barrier_semaphore()
     greeted = [(sp, right), (sp, left), (sp, partner)] + [(span, tp) for span in nexts]
-    for number in range(ROUNDS):
-        greeted.append(((sp + 2 ** number) % SPANS, tp))
-        if number < ROUNDS - 1:
-            greeted.append(((sp + SPANS - 2 ** number) % SPANS, tp))
     for span, seat in greeted:
         pl.semaphore_signal(barrier, inc=1, device_id=(span, seat), device_id_type=MESH)
 
@@ -105,8 +101,6 @@
     for load in out_loads:
         load.start()
 
-    pl.semaphore_wait(barrier, len(greeted))
-
     def piece(seat, half):
         return xg.at[seat, pl.ds(half * half_rows, half_rows), :]
 
@@ -129,6 +123,7 @@
         12: gather(12, piece(across, 1), partner),
     }
     own_load.wait()
+    pl.semaphore_wait(barrier, len(greeted))
     for number in (0, 2, 1, 3, 4):
         sends[number].start()
 
@@ -269,11 +264,16 @@
     st_out[0, 0:HEAD, :] = jnp.where(low_square, outer[:HEAD], outer[HEAD:])
     st_out[0, HEAD:HEAD + 8, :] = tail(
         jnp.sum(end_weights * key_floats, axis=0, keepdims=True), span_top, span_decay)
-    st_before[0:HEAD, :] = jnp.zeros((HEAD, 128), F32)
-    st_before[HEAD:HEAD + 8, :] = tail(0.0, NEGATIVE, 0.0) + jnp.zeros((8, 128), F32)
+    for kind in range(2):
+        st_before[kind, 0:HEAD, :] = jnp.zeros((HEAD, 128), F32)
+        st_before[kind, HEAD:HEAD + 8, :] = tail(0.0, NEGATIVE, 0.0) + jnp.zeros((8, 128), F32)
+
+    def rise(number):
+        return jnp.where(number == 2, 1, jnp.where(number == 3, 2, 4))
 
     def scan_copy(number):
-        target = (sp + lax.shift_left(jnp.int32(1), jnp.int32(number))) % SPANS
+        beside = jnp.where(number == 0, across_x + 1 - 2 * (across_x % 2), (across_x + 2) % 4)
+        target = jnp.where(number < 2, 4 * z + beside, 4 * ((z + rise(number)) % 8) + across_x)
         return remote(st_out.at[number], st_in.at[number], scan_send.at[number],
                       scan_recv.at[number], target, tp)
 
@@ -343,20 +343,26 @@
         scan_copy(number).wait_recv()
         memory = st_in[number, 0:HEAD, :]
         ending = st_in[number, HEAD:HEAD + 8, :]
-
-        @pl.when(sp >= lax.shift_left(jnp.int32(1), jnp.int32(number)))
+        in_row = number < 2
+        later_half = jnp.where(number == 0, across_x % 2, across_x // 2)
+        earlier = jnp.where(in_row, later_half, jnp.where(z >= rise(number), 1, 0)) > 0
+        kind = jnp.where(in_row, 0, 1)
+
+        @pl.when(earlier)
         def _():
-            done = joined((memory, ending), (st_before[0:HEAD, :], st_before[HEAD:HEAD + 8, :]))
-            st_before[0:HEAD, :] = done[0]
-            st_before[HEAD:HEAD + 8, :] = done[1]
+            done = joined((memory, ending),
+                          (st_before[kind, 0:HEAD, :], st_before[kind, HEAD:HEAD + 8, :]))
+            st_before[kind, 0:HEAD, :] = done[0]
+            st_before[kind, HEAD:HEAD + 8, :] = done[1]
 
         @pl.when(number < ROUNDS - 1)
         def _():
             mine = (st_out[number, 0:HEAD, :], st_out[number, HEAD:HEAD + 8, :])
-            whole = joined((memory, ending), mine)
-            reached = sp >= lax.shift_left(jnp.int32(1), jnp.int32(number))
-            st_out[number + 1, 0:HEAD, :] = jnp.where(reached, whole[0], mine[0])
-            st_out[number + 1, HEAD:HEAD + 8, :] = jnp.where(reached, whole[1], mine[1])
+            after = joined((memory, ending), mine)
+            ahead = joined(mine, (memory, ending))
+            for place, (one, two, same) in enumerate(zip(after, ahead, mine)):
+                merged = jnp.where(earlier, one, jnp.where(in_row, two, same))
+                st_out[number + 1, HEAD * place:HEAD + 8 * place, :] = merged
 
     def attend(ring, dz, dx, valid):
         origin = span_at(dz, dx)
@@ -421,7 +427,8 @@
         def _():
             x_copy(5, 2, 0, 0).wait_recv()
             x_copy(5, 3, 0, 0).wait_recv()
-            z_copy(4, 0, 1, 2).start()
+            for way in range(2):
+                z_copy(4, way, 1, 2).start()
 
         def chain(number, way, dx, last):
             @pl.when(hop <= last)
@@ -434,30 +441,11 @@
 
         first = 1 + 2 * pair
 
-        def first_downwards():
-            chain(first, 1, pair, 4)
-
-            @pl.when(pair == 1)
-            def _():
-                x_copy(9 + hop, 3, 0, hop).start()
-
-        def second_downwards():
-            @pl.when(pair == 0)
-            def _():
-                chain(2, 1, 3, 4)
-                x_copy(9 + hop, 2, 0, hop).start()
-
-            @pl.when((pair == 1) & (hop >= 2))
-            def _():
-                for kind in (2, 3):
-                    x_copy(8 + hop, kind, 0, hop - 1).wait_recv()
-
-        by_way(lambda: chain(first, 0, pair, 3), first_downwards,
-               lambda way: attend(0, signed(way, hop), pair, hop <= 3 + way))
+        by_way(lambda: chain(first, 0, pair, 4), lambda: chain(first, 1, pair, 3),
+               lambda way: attend(0, signed(way, hop), pair, hop <= 4 - way))
         by_way(lambda: x_arrival(1, 0), lambda: x_arrival(1, 1), lambda side: x_attend(1, side))
-        by_way(lambda: chain(first + 1, 0, 3 - pair, 3), second_downwards,
-               lambda way: attend(0, signed(way, hop - pair * way), 3 - pair,
-                                  (hop >= 1 + pair * way) & (hop <= 3 + way)))
+        by_way(lambda: chain(first + 1, 0, 3 - pair, 3), lambda: chain(first + 1, 1, 3 - pair, 4),
+               lambda way: attend(0, signed(way, hop), 3 - pair, hop <= 3 + way))
 
         def relayed(rows_way):
             j = i - 1
@@ -494,19 +482,13 @@
         return unused
 
     lax.fori_loop(0, 8, iteration, 0)
-    for kind in (2, 3):
-        x_copy(13, kind, 0, 4).wait_recv()
-    attend(0, 4, 2, sp >= 0)
-    for number, lasts in enumerate(((4, 3), (3, 4), (3, 4), (3, 4), (3, 0))):
+    for number, lasts in enumerate(((4, 3), (4, 3), (3, 4), (4, 3), (3, 4))):
         for way, last in enumerate(lasts):
             for hop in range(1, last + 1):
                 z_copy(number, way, hop, 0).wait_send()
     for number in range(9):
         for kind in range(4):
             x_copy(number, kind, 1, 0).wait_send()
-    for number in range(10, 14):
-        for kind in (2, 3):
-            x_copy(number, kind, 0, 0).wait_send()
     for number in range(ROUNDS):
         scan_copy(number).wait_send()
 
@@ -525,7 +507,9 @@
 
     start_memory = jnp.zeros((HEAD, 128), F32)
     start_tail = jnp.zeros((8, 128), F32)
-    entered = joined((start_memory, start_tail), (st_before[0:HEAD, :], st_before[HEAD:HEAD + 8, :]))
+    entered = (start_memory, start_tail)
+    for kind in (1, 0):
+        entered = joined(entered, (st_before[kind, 0:HEAD, :], st_before[kind, HEAD:HEAD + 8, :]))
     memory_in, normal_in, stable_in = entered[0], entered[1][0:1], entered[1][1:2]
     spread = jnp.concatenate(
         [jnp.where(low_square, memory_in, 0.0), jnp.where(low_square, 0.0, memory_in)], axis=0)
@@ -658,7 +642,7 @@
         pltpu.VMEM((2, 2 * rows, 128), F32),
         pltpu.VMEM((ROUNDS, HEAD + 8, 128), F32),
         pltpu.VMEM((ROUNDS, HEAD + 8, 128), F32),
-        pltpu.VMEM((HEAD + 8, 128), F32),
+        pltpu.VMEM((2, HEAD + 8, 128), F32),
         pltpu.VMEM((2, rows, 128), F32),
         pltpu.VMEM((rows, 128), F32),
         pltpu.VMEM((rows, 256), BF16),
@@ -672,8 +656,8 @@
         pltpu.SemaphoreType.DMA((13,)),
         pltpu.SemaphoreType.DMA((5, 2, 4)),
         pltpu.SemaphoreType.DMA((5, 2, 4)),
-        pltpu.SemaphoreType.DMA((14, 4)),
-        pltpu.SemaphoreType.DMA((14, 4)),
+        pltpu.SemaphoreType.DMA((10, 4)),
+        pltpu.SemaphoreType.DMA((10, 4)),
         pltpu.SemaphoreType.DMA((ROUNDS,)),
         pltpu.SemaphoreType.DMA((ROUNDS,)),
         pltpu.SemaphoreType.DMA((4,)),

time: 89.6 us -> 86.3 us (0.963)
  the two profiles are of different devices: /device:TPU:225 before, /device:TPU:1 now
where the time goes in v4:
time: 86.3 us; the launch traced here: 85 us
  Pallas kernels  83.4 us (97%)
  local copies, waits for them, and re-layouts  1.62 us (2%)
    pallas_call x1, Pallas kernels, per_device(): pl.pallas_call(layer_kernel, out_shape=jax.ShapeDtypeStruct((rows, column...  83.4 us

profile of v4, /device:TPU:1, one launch (start us, length us, event | category | flops | bytes accessed | tf_op | source)
XLA Modules:
  0.0 85.0 jit_solution(8909036897583682333)
XLA Ops:
  0.0 83.4 %layer.1 = bf16[384,256]{1,0:T(8,128)(2,1)} custom-call(bf16[384,256]{1,0:T(8,128)(2,1)} %x.1, f32[8,1,256]{2,1,0:T(1,128)} %bitcast.5, f32[2,384,128]{2,1,0:T(8,128)} %constant.4.clone.near_in, f32[32,2,128]{2,1,0:T(2,128)} %constant.5.clone.far_in, bf16[2048,128]{1,0:T(8,128)(2,1)} %wq.1, bf16[2048,128]{1,0:T(8,128)(2,1)} %wk.1, bf16[2048,128]{1,0:T(8,128)(2,1)} %wv.1, ...), custom_call_target="tpu_custom_call" | custom-call | tf_op jit(solution)/shard_map/layer/pallas_call | solution.py:668
  83.4 1.6 %copy.20 = bf16[384,256]{1,0:T(8,128)(2,1)} copy(bf16[384,256]{1,0:T(8,128)(2,1)} %layer.1) | data formatting | bytes 393216

commit v5 on v4

--- a/solution.py
+++ b/solution.py
@@ -14,8 +14,8 @@
 LOG2E = 1.4426950408889634
 SPANS = 32
 ROUNDS = 5
-X_LAG = 2
-RELAY_LAG = 1
+X_LAG = 1
+RELAY_LAG = 0
 MESH = pl.DeviceIdType.MESH
 F32 = jnp.float32
 BF16 = jnp.bfloat16
@@ -101,31 +101,46 @@
     for load in out_loads:
         load.start()
 
-    def piece(seat, half):
-        return xg.at[seat, pl.ds(half * half_rows, half_rows), :]
-
-    def gather(number, ref, seat):
-        return remote(ref, ref, gather_send.at[number], gather_recv.at[number], sp, seat)
+    quarter = half_rows // 2
+
+    def piece(seat, half, part=None):
+        if part is None:
+            return xg.at[seat, pl.ds(half * half_rows, half_rows), :]
+        return xg.at[seat, pl.ds(half * half_rows + part * quarter, quarter), :]
+
+    def gather(number, seat, goal, half=None):
+        if half is None:
+            ref = xg.at[seat]
+            return [remote(ref, ref, gather_send.at[number, 0], gather_recv.at[number, 0], sp, goal)]
+        if number in (1, 3, 6, 8, 9, 10):
+            ref = piece(seat, half)
+            return [remote(ref, ref, gather_send.at[number, 0], gather_recv.at[number, 0], sp, goal)]
+        refs = [piece(seat, half, part) for part in range(2)]
+        return [remote(ref, ref, gather_send.at[number, part], gather_recv.at[number, part], sp, goal)
+                for part, ref in enumerate(refs)]
 
     sends = {
-        0: gather(0, piece(tp, 0), right),
-        1: gather(1, piece(tp, 1), right),
-        2: gather(2, piece(tp, 1), left),
-        3: gather(3, piece(tp, 0), left),
-        4: gather(4, xg.at[tp], partner),
-        5: gather(5, piece(left, 0), right),
-        6: gather(6, piece(left, 0), partner),
-        7: gather(7, piece(right, 1), left),
-        8: gather(8, piece(right, 1), partner),
-        9: gather(9, piece(left, 1), partner),
-        10: gather(10, piece(right, 0), partner),
-        11: gather(11, piece(across, 0), partner),
-        12: gather(12, piece(across, 1), partner),
+        0: gather(0, tp, right, 0),
+        1: gather(1, tp, right, 1),
+        2: gather(2, tp, left, 1),
+        3: gather(3, tp, left, 0),
+        4: gather(4, tp, partner),
+        5: gather(5, left, right, 0),
+        6: gather(6, left, partner, 0),
+        7: gather(7, right, left, 1),
+        8: gather(8, right, partner, 1),
+        9: gather(9, left, partner, 1),
+        10: gather(10, right, partner, 0),
+        11: gather(11, across, partner, 0),
+        12: gather(12, across, partner, 1),
     }
     own_load.wait()
     pl.semaphore_wait(barrier, len(greeted))
-    for number in (0, 2, 1, 3, 4):
-        sends[number].start()
+    for part in range(2):
+        sends[0][part].start()
+        sends[2][part].start()
+    for number in (1, 3, 4):
+        sends[number][0].start()
 
     def absorb(seat):
         block = xg[seat].astype(F32)
@@ -135,34 +150,38 @@
     squares[...] = jnp.zeros_like(squares)
     small_loads[0].wait()
     absorb(tp)
-    sends[0].wait_recv()
-    sends[5].start()
-    sends[6].start()
-    sends[2].wait_recv()
-    sends[7].start()
-    sends[8].start()
-    sends[4].wait_recv()
+    for part in range(2):
+        sends[0][part].wait_recv()
+        sends[5][part].start()
+        sends[2][part].wait_recv()
+        sends[7][part].start()
+    sends[6][0].start()
+    sends[8][0].start()
+    sends[4][0].wait_recv()
     absorb(partner)
-    sends[1].wait_recv()
-    sends[9].start()
-    sends[3].wait_recv()
-    sends[10].start()
+    sends[1][0].wait_recv()
+    sends[9][0].start()
+    sends[3][0].wait_recv()
+    sends[10][0].start()
     absorb(left)
     absorb(right)
-    sends[5].wait_recv()
-    sends[11].start()
-    sends[7].wait_recv()
-    sends[12].start()
+    for part in range(2):
+        sends[5][part].wait_recv()
+        sends[11][part].start()
+        sends[7][part].wait_recv()
+        sends[12][part].start()
     for number in (6, 8, 9, 10):
-        sends[number].wait_recv()
+        sends[number][0].wait_recv()
     absorb(2 * ((y + 1) % 4) + 1 - c)
     absorb(2 * ((y + 3) % 4) + 1 - c)
     absorb(across)
-    sends[11].wait_recv()
-    sends[12].wait_recv()
+    for part in range(2):
+        sends[11][part].wait_recv()
+        sends[12][part].wait_recv()
     absorb(2 * ((y + 2) % 4) + 1 - c)
     for number in range(13):
-        sends[number].wait_send()
+        for copy in sends[number]:
+            copy.wait_send()
     for load in loads + [small_loads[number] for number in range(1, 9)]:
         load.wait()
 
@@ -287,11 +306,13 @@
                 tail(first * old[0:1] + second * new[0:1], highest, old[2:3] + decays))
 
     scale = DD ** (-0.5) * LOG2E
-    ones_low = low
-
-    def visit(ring, position, mask=None):
+
+    def visit(ring, position, mask=None, other=None):
         block = held[ring, position]
-        extended = jnp.where(ones_low, jnp.ones_like(block), block)
+        if other is not None:
+            block = jnp.concatenate([block, held[ring, other]], axis=0)
+        some = lax.broadcasted_iota(jnp.int32, block.shape, 1) < HEAD
+        extended = jnp.where(some, jnp.ones_like(block), block)
         scores = dot_t(qs[ring], block)
         if mask is not None:
             scores = jnp.where(mask, scores, NEGATIVE)
@@ -300,7 +321,7 @@
             old = top[ring]
             highest = jnp.maximum(old, jnp.max(scores, axis=1, keepdims=True))
         shift = highest * scale
-        weights = jnp.exp2(scores * scale - jnp.concatenate([shift] * (rows // 128), axis=1))
+        weights = jnp.exp2(scores * scale - jnp.concatenate([shift] * (block.shape[0] // 128), axis=1))
         product = dot(weights.astype(BF16), extended)
         if mask is not None:
             acc[ring] = product
@@ -364,7 +385,19 @@
                 merged = jnp.where(earlier, one, jnp.where(in_row, two, same))
                 st_out[number + 1, HEAD * place:HEAD + 8 * place, :] = merged
 
-    def attend(ring, dz, dx, valid):
+    def attend(ring, pair):
+        spans = [span_at(dz, dx) for dz, dx, _ in pair]
+        counts = [valid & (span < sp) for span, (_, _, valid) in zip(spans, pair)]
+
+        @pl.when(counts[0] & counts[1])
+        def _():
+            visit(ring, spans[0], other=spans[1])
+
+        @pl.when(counts[0] != counts[1])
+        def _():
+            visit(ring, jnp.where(counts[0], spans[0], spans[1]))
+
+    def attend_one(ring, dz, dx, valid):
         origin = span_at(dz, dx)
 
         @pl.when(valid & (origin < sp))
@@ -373,18 +406,6 @@
 
     def iteration(i, unused):
         pair, hop = i % 2, i // 2 + 1
-
-        def by_way(ups, downs, then):
-            def body(way, unused):
-                pl.when(way == 0)(ups)
-                pl.when(way == 1)(downs)
-                then(way)
-                return unused
-
-            lax.fori_loop(0, 2, body, 0)
-
-        def signed(way, distance):
-            return (2 * way - 1) * distance
 
         @pl.when((i >= 1) & (i < ROUNDS))
         def _():
@@ -404,8 +425,9 @@
                 for kind in range(2):
                     x_copy(5 * way + i + 1, kind, 1, (2 * way - 1) * (i + 1)).start()
 
-        by_way(lambda: own_chain(0), lambda: own_chain(1),
-               lambda way: attend(1, signed(way, i + 1), 0, i < 4 - way))
+        own_chain(0)
+        own_chain(1)
+        attend(1, ((-i - 1, 0, i < 4), (i + 1, 0, i < 3)))
 
         def x_arrival(rows_way, kind):
             valid = (i <= 4) if rows_way == 0 else (i >= 1) & (i <= 3)
@@ -416,12 +438,15 @@
                 x_copy(5 * rows_way + i, kind, 1, dz).wait_recv()
                 x_copy(5 * rows_way + i, kind + 2, 1, dz).start()
 
-        def x_attend(rows_way, side):
+        def x_attend(rows_way):
             j = i - X_LAG
             valid = (j >= 0) & (j <= 4) if rows_way == 0 else (j >= 1) & (j <= 3)
-            attend(1, (2 * rows_way - 1) * j, 3 - 2 * side, valid)
-
-        by_way(lambda: x_arrival(0, 0), lambda: x_arrival(0, 1), lambda side: x_attend(0, side))
+            dz = (2 * rows_way - 1) * j
+            attend(1, ((dz, 3, valid), (dz, 1, valid)))
+
+        x_arrival(0, 0)
+        x_arrival(0, 1)
+        x_attend(0)
 
         @pl.when(i == 0)
         def _():
@@ -441,11 +466,15 @@
 
         first = 1 + 2 * pair
 
-        by_way(lambda: chain(first, 0, pair, 4), lambda: chain(first, 1, pair, 3),
-               lambda way: attend(0, signed(way, hop), pair, hop <= 4 - way))
-        by_way(lambda: x_arrival(1, 0), lambda: x_arrival(1, 1), lambda side: x_attend(1, side))
-        by_way(lambda: chain(first + 1, 0, 3 - pair, 3), lambda: chain(first + 1, 1, 3 - pair, 4),
-               lambda way: attend(0, signed(way, hop), 3 - pair, hop <= 3 + way))
+        chain(first, 0, pair, 4)
+        chain(first, 1, pair, 3)
+        attend(0, ((-hop, pair, hop <= 4), (hop, pair, hop <= 3)))
+        x_arrival(1, 0)
+        x_arrival(1, 1)
+        x_attend(1)
+        chain(first + 1, 0, 3 - pair, 3)
+        chain(first + 1, 1, 3 - pair, 4)
+        attend(0, ((-hop, 3 - pair, hop <= 3), (hop, 3 - pair, hop <= 4)))
 
         def relayed(rows_way):
             j = i - 1
@@ -456,20 +485,11 @@
                 for kind in (2, 3):
                     x_copy(5 * rows_way + j, kind, 1, (2 * rows_way - 1) * j).wait_recv()
 
-        def relay_attend(way):
-            j = i - 1 - RELAY_LAG
-            own = way == 2
-            valid = jnp.where(own, i < 3, (j >= way) & (j <= 4 - way))
-            attend(jnp.where(own, 0, 1), jnp.where(own, 0, signed(way, j)),
-                   jnp.where(own, 3 - i, 2), valid)
-
-        def body(way, unused):
-            pl.when(way == 0)(lambda: relayed(0))
-            pl.when(way == 1)(lambda: relayed(1))
-            relay_attend(way)
-            return unused
-
-        lax.fori_loop(0, 3, body, 0)
+        relayed(0)
+        relayed(1)
+        j = i - 1 - RELAY_LAG
+        attend(1, ((-j, 2, (j >= 0) & (j <= 4)), (j, 2, (j >= 1) & (j <= 3))))
+        attend_one(0, 0, 3 - i, i < 3)
 
         @pl.when(i == 0)
         def _():
@@ -544,8 +564,6 @@
         own = share(2 * ((y + offsets[number]) % 4) + c).astype(F32)
         pairs[number].wait_recv()
         return own + from_partner[number].astype(F32)
-
-    quarter = half_rows // 2
 
     def shift(number, seat, part=None):
         if part is None:
@@ -652,8 +670,8 @@
         pltpu.VMEM((6, half, 256), BF16),
         pltpu.SemaphoreType.DMA((9,)),
         pltpu.SemaphoreType.DMA((25,)),
-        pltpu.SemaphoreType.DMA((13,)),
-        pltpu.SemaphoreType.DMA((13,)),
+        pltpu.SemaphoreType.DMA((13, 2)),
+        pltpu.SemaphoreType.DMA((13, 2)),
         pltpu.SemaphoreType.DMA((5, 2, 4)),
         pltpu.SemaphoreType.DMA((5, 2, 4)),
         pltpu.SemaphoreType.DMA((10, 4)),

time: 86.3 us -> 84.6 us (0.980); the launches traced: 85 us -> 84.5 us
  no operation moved by 1% of the time
where the time goes in v5:
time: 84.6 us; the launch traced here: 84.5 us
  Pallas kernels  82.9 us (98%)
  local copies, waits for them, and re-layouts  1.62 us (2%)
    pallas_call x1, Pallas kernels, per_device(): pl.pallas_call(layer_kernel, out_shape=jax.ShapeDtypeStruct((rows, column...  82.9 us

profile of v5, /device:TPU:1, one launch (start us, length us, event | category | flops | bytes accessed | tf_op | source)
XLA Modules:
  0.0 84.5 jit_solution(7422679020563311265)
XLA Ops:
  0.0 82.9 %layer.1 = bf16[384,256]{1,0:T(8,128)(2,1)} custom-call(bf16[384,256]{1,0:T(8,128)(2,1)} %x.1, f32[8,1,256]{2,1,0:T(1,128)} %bitcast.5, f32[2,384,128]{2,1,0:T(8,128)} %constant.4.clone.near_in, f32[32,2,128]{2,1,0:T(2,128)} %constant.5.clone.far_in, bf16[2048,128]{1,0:T(8,128)(2,1)} %wq.1, bf16[2048,128]{1,0:T(8,128)(2,1)} %wk.1, bf16[2048,128]{1,0:T(8,128)(2,1)} %wv.1, ...), custom_call_target="tpu_custom_call" | custom-call | tf_op jit(solution)/shard_map/layer/pallas_call | solution.py:686
  82.9 1.6 %copy.20 = bf16[384,256]{1,0:T(8,128)(2,1)} copy(bf16[384,256]{1,0:T(8,128)(2,1)} %layer.1) | data formatting | bytes 393216

commit v6 on v5

--- a/solution.py
+++ b/solution.py
@@ -14,7 +14,7 @@
 LOG2E = 1.4426950408889634
 SPANS = 32
 ROUNDS = 5
-X_LAG = 1
+X_LAG = 0
 RELAY_LAG = 0
 MESH = pl.DeviceIdType.MESH
 F32 = jnp.float32
@@ -237,73 +237,8 @@
         for side in range(2):
             inside = (lane >= DD * side) & (lane < DD * side + DD)
             qs[head, side * rows:(side + 1) * rows, :] = jnp.where(inside, turned, 0.0).astype(BF16)
-    product = dot(scaled, w[2]) * inverse
-    mk[...] = product[:, :128].astype(BF16)
-    mv[...] = product[:, 128:].astype(BF16)
-    inverse_row = jnp.transpose(jnp.broadcast_to(inverse, (rows, 128)))[0:1, :]
-    gate_in = dot_t(wig[...], scaled) * inverse_row
-    forget = dot_t(wfg[...], scaled) * inverse_row
-
-    def log_sigmoid(a):
-        return jnp.minimum(a, 0.0) - jnp.log1p(jnp.exp(-jnp.abs(a)))
-
-    def per_head(parts):
-        return jnp.where(low, parts[0], parts[1])
-
-    first_row = lax.broadcasted_iota(jnp.int32, (2, rows), 0) == 0
-    log_forget = log_sigmoid(forget + jnp.where(first_row, bias[0], bias[1])) + decay[...]
     before_or_at = (lax.broadcasted_iota(jnp.int32, (rows, rows), 1)
                     <= lax.broadcasted_iota(jnp.int32, (rows, rows), 0))
-    triangle = jnp.where(before_or_at, 1.0, 0.0).astype(BF16)
-    high, middle, small = thirds(log_forget)
-    cumulative = dot_t(high, triangle) + dot_t(middle, triangle) + dot_t(small, triangle)
-    gate_rows[...] = gate_in - cumulative
-    upper_rows = lax.broadcasted_iota(jnp.int32, (128, rows), 0) < HEAD
-
-    def columns(pair):
-        return jnp.transpose(jnp.where(upper_rows, pair[0:1, :], pair[1:2, :]))
-
-    gates[0] = columns(cumulative)
-    gates[1] = columns(gate_rows[...])
-    span_decay = gates[0, rows - 1:rows, :]
-    toward_end = span_decay + gates[1]
-    span_top = jnp.max(toward_end, axis=0, keepdims=True)
-    end_weights = jnp.exp(toward_end - span_top)
-    key_floats = mk[...].astype(F32) * 0.125
-    weighted = jnp.transpose(end_weights * mv[...].astype(F32))
-    high, small = halves(weighted)
-    keys_exact = key_floats.astype(BF16)
-    outer = dot(high, keys_exact) + dot(small, keys_exact)
-    row = lax.broadcasted_iota(jnp.int32, (8, 128), 0)
-
-    def tail(normal, stable, decays):
-        return jnp.where(row == 0, normal, jnp.where(row == 1, stable, decays))
-
-    low_square = low[:HEAD]
-    st_out[0, 0:HEAD, :] = jnp.where(low_square, outer[:HEAD], outer[HEAD:])
-    st_out[0, HEAD:HEAD + 8, :] = tail(
-        jnp.sum(end_weights * key_floats, axis=0, keepdims=True), span_top, span_decay)
-    for kind in range(2):
-        st_before[kind, 0:HEAD, :] = jnp.zeros((HEAD, 128), F32)
-        st_before[kind, HEAD:HEAD + 8, :] = tail(0.0, NEGATIVE, 0.0) + jnp.zeros((8, 128), F32)
-
-    def rise(number):
-        return jnp.where(number == 2, 1, jnp.where(number == 3, 2, 4))
-
-    def scan_copy(number):
-        beside = jnp.where(number == 0, across_x + 1 - 2 * (across_x % 2), (across_x + 2) % 4)
-        target = jnp.where(number < 2, 4 * z + beside, 4 * ((z + rise(number)) % 8) + across_x)
-        return remote(st_out.at[number], st_in.at[number], scan_send.at[number],
-                      scan_recv.at[number], target, tp)
-
-    def joined(earlier, later):
-        old, new = earlier[1], later[1]
-        decays, stable, later_stable = new[2:3], old[1:2], new[1:2]
-        highest = jnp.maximum(decays + stable, later_stable)
-        first = jnp.exp(decays + stable - highest)
-        second = jnp.exp(later_stable - highest)
-        return (first * earlier[0] + second * later[0],
-                tail(first * old[0:1] + second * new[0:1], highest, old[2:3] + decays))
 
     scale = DD ** (-0.5) * LOG2E
 
@@ -331,7 +266,35 @@
 
     causal = jnp.concatenate([before_or_at, before_or_at], axis=0)
     visit(0, sp, causal)
-    scan_copy(0).start()
+    visit(1, sp, causal)
+
+    product = dot(scaled, w[2]) * inverse
+    mk[...] = product[:, :128].astype(BF16)
+    mv[...] = product[:, 128:].astype(BF16)
+    inverse_row = jnp.transpose(jnp.broadcast_to(inverse, (rows, 128)))[0:1, :]
+    gate_weights = jnp.concatenate([wig[...].astype(F32), wfg[...].astype(F32)], axis=0)
+    both_gates = dot_t(gate_weights.astype(BF16), scaled) * inverse_row
+    gate_in, forget = both_gates[0:2], both_gates[2:4]
+
+    def log_sigmoid(a):
+        return jnp.minimum(a, 0.0) - jnp.log1p(jnp.exp(-jnp.abs(a)))
+
+    def per_head(parts):
+        return jnp.where(low, parts[0], parts[1])
+
+    first_row = lax.broadcasted_iota(jnp.int32, (2, rows), 0) == 0
+    log_forget = log_sigmoid(forget + jnp.where(first_row, bias[0], bias[1])) + decay[...]
+    triangle = jnp.where(before_or_at, 1.0, 0.0).astype(BF16)
+    high, middle, small = thirds(log_forget)
+    cumulative = dot_t(high, triangle) + dot_t(middle, triangle) + dot_t(small, triangle)
+    gate_rows[...] = gate_in - cumulative
+    upper_rows = lax.broadcasted_iota(jnp.int32, (128, rows), 0) < HEAD
+
+    def columns(pair):
+        return jnp.transpose(jnp.where(upper_rows, pair[0:1, :], pair[1:2, :]))
+
+    gates[0] = columns(cumulative)
+    gates[1] = columns(gate_rows[...])
     x_copy(5, 0, 0, 0).wait_recv()
     x_copy(5, 2, 0, 0).start()
     for way in range(2):
@@ -340,7 +303,47 @@
     x_copy(5, 3, 0, 0).start()
     for way in range(2):
         z_copy(3, way, 1, 1).start()
-    visit(1, sp, causal)
+    span_decay = gates[0, rows - 1:rows, :]
+    toward_end = span_decay + gates[1]
+    span_top = jnp.max(toward_end, axis=0, keepdims=True)
+    end_weights = jnp.exp(toward_end - span_top)
+    key_floats = mk[...].astype(F32) * 0.125
+    weighted = jnp.transpose(end_weights * mv[...].astype(F32))
+    high, small = halves(weighted)
+    keys_exact = key_floats.astype(BF16)
+    outer = dot(high, keys_exact) + dot(small, keys_exact)
+    row = lax.broadcasted_iota(jnp.int32, (8, 128), 0)
+
+    def tail(normal, stable, decays):
+        return jnp.where(row == 0, normal, jnp.where(row == 1, stable, decays))
+
+    low_square = low[:HEAD]
+    st_out[0, 0:HEAD, :] = jnp.where(low_square, outer[:HEAD], outer[HEAD:])
+    st_out[0, HEAD:HEAD + 8, :] = tail(
+        jnp.sum(end_weights * key_floats, axis=0, keepdims=True), span_top, span_decay)
+    for kind in range(2):
+        st_before[kind, 0:HEAD, :] = jnp.zeros((HEAD, 128), F32)
+        st_before[kind, HEAD:HEAD + 8, :] = tail(0.0, NEGATIVE, 0.0) + jnp.zeros((8, 128), F32)
+
+    def rise(number):
+        return jnp.where(number == 2, 1, jnp.where(number == 3, 2, 4))
+
+    def scan_copy(number):
+        beside = jnp.where(number == 0, across_x + 1 - 2 * (across_x % 2), (across_x + 2) % 4)
+        target = jnp.where(number < 2, 4 * z + beside, 4 * ((z + rise(number)) % 8) + across_x)
+        return remote(st_out.at[number], st_in.at[number], scan_send.at[number],
+                      scan_recv.at[number], target, tp)
+
+    def joined(earlier, later):
+        old, new = earlier[1], later[1]
+        decays, stable, later_stable = new[2:3], old[1:2], new[1:2]
+        highest = jnp.maximum(decays + stable, later_stable)
+        first = jnp.exp(decays + stable - highest)
+        second = jnp.exp(later_stable - highest)
+        return (first * earlier[0] + second * later[0],
+                tail(first * old[0:1] + second * new[0:1], highest, old[2:3] + decays))
+
+    scan_copy(0).start()
 
     def local_memory():
         sums, tops, totals = [], [], []

time: 84.6 us -> 82.3 us (0.973)
  Pallas kernels: 82.9 us -> 80.6 us
    pallas_call x1, Pallas kernels: 82.9 us -> 80.6 us  [per_device(): pl.pallas_call(layer_kernel, out_shape=jax.ShapeDtypeStruct((rows, column...]
where the time goes in v6:
time: 82.3 us; the launch traced here: 82.2 us
  Pallas kernels  80.6 us (98%)
  local copies, waits for them, and re-layouts  1.62 us (2%)
    pallas_call x1, Pallas kernels, per_device(): pl.pallas_call(layer_kernel, out_shape=jax.ShapeDtypeStruct((rows, column...  80.6 us

profile of v6, /device:TPU:1, one launch (start us, length us, event | category | flops | bytes accessed | tf_op | source)
XLA Modules:
  0.0 82.2 jit_solution(7917234902038530741)
XLA Ops:
  0.0 80.6 %layer.1 = bf16[384,256]{1,0:T(8,128)(2,1)} custom-call(bf16[384,256]{1,0:T(8,128)(2,1)} %x.1, f32[8,1,256]{2,1,0:T(1,128)} %bitcast.5, f32[2,384,128]{2,1,0:T(8,128)} %constant.4.clone.near_in, f32[32,2,128]{2,1,0:T(2,128)} %constant.5.clone.far_in, bf16[2048,128]{1,0:T(8,128)(2,1)} %wq.1, bf16[2048,128]{1,0:T(8,128)(2,1)} %wk.1, bf16[2048,128]{1,0:T(8,128)(2,1)} %wv.1, ...), custom_call_target="tpu_custom_call" | custom-call | tf_op jit(solution)/shard_map/layer/pallas_call | solution.py:689
  80.6 1.6 %copy.20 = bf16[384,256]{1,0:T(8,128)(2,1)} copy(bf16[384,256]{1,0:T(8,128)(2,1)} %layer.1) | data formatting | bytes 393216
